TPU v7x, 128 devices: a whole 4x4x4 slice. The times are simulated.
128 devices in a mesh: kv: 32 (over z, y, core), tp: 4 (over x).
Axes of the slice: x: 4, y: 4, z: 4, core: 2. Of those that a mesh axis runs over, the one named last changes fastest.
Arguments:
- tokens: bfloat16 [512, 4, 4096], P('kv'), may hold values from -6 to 6
- norm_gain: bfloat16 [4096], replicated, may hold values from 0.099609375 to 1.8984375
- query_weight: bfloat16 [4096, 2048], P(None, 'tp'), may hold values from -0.09375 to 0.09375
- key_weight: bfloat16 [4096, 2048], P(None, 'tp'), may hold values from -0.09375 to 0.09375
- value_weight: bfloat16 [4096, 2048], P(None, 'tp'), may hold values from -0.09375 to 0.09375
- outgate_weight: bfloat16 [4096, 2048], P(None, 'tp'), may hold values from -0.09375 to 0.09375
- gate_weight: bfloat16 [4096, 32], replicated, may hold values from -0.09375 to 0.09375
- gate_bias: float32 [2, 16], replicated, may hold values from -1 to 4
- head_gain: bfloat16 [2048], P('tp'), may hold values from 0.099609375 to 1.8984375
- out_weight: bfloat16 [2048, 4096], P('tp', 'kv'), may hold values from -0.125 to 0.125
- state_c: float32 [512, 16, 128, 128], P('kv', 'tp'), may hold values from -3 to 3
- state_n: float32 [512, 16, 128], P('kv', 'tp'), may hold values from -3 to 3
- state_m: float32 [512, 16], P('kv', 'tp'), may hold values from -1 to 2
- prev_keys: bfloat16 [512, 16, 4, 128], P('kv', 'tp'), may hold values from -6 to 6
- prev_values: bfloat16 [512, 16, 4, 128], P('kv', 'tp'), may hold values from -6 to 6
- prev_gates: float32 [512, 16, 2, 4], P('kv', 'tp'), may hold values from -2 to 5
- accepted: int32 [512], P('kv'), may hold values from 0 to 4
Outputs:
- mixed: bfloat16 [512, 4, 4096], P(None, None, 'kv')
- carried_c: float32 [512, 16, 128, 128], P('kv', 'tp')
- carried_n: float32 [512, 16, 128], P('kv', 'tp')
- carried_m: float32 [512, 16], P('kv', 'tp')
- step_keys: bfloat16 [512, 16, 4, 128], P('kv', 'tp')
- step_values: bfloat16 [512, 16, 4, 128], P('kv', 'tp')
- step_gates: float32 [512, 16, 2, 4], P('kv', 'tp')
Inputs may be any that keep to these rules, and one draw needn't show every extreme that they name: accepted counts proposals of the last step, from none to all 4.
All inputs are finite; a program needn't handle non-finite values.
Results may differ from a plain program's by a relative error of at most 0.0075.
The roundings to bfloat16 on the way count: a program that leaves them out, or rounds other values in their place, can miss the bound.
Values may be sent and summed in bfloat16 or wider, within the bound.
No kernel may reach another device: no remote copies, remote signals or barrier semaphores. Data moves between devices by JAX's collectives and lax.ppermute only.
A program may use at most 128 MiB of HBM per device.

v0:
```python
import jax
import jax.numpy as jnp
from jax import lax
from jax.sharding import PartitionSpec as P

EPSILON = 1e-06
HIGHEST = lax.Precision.HIGHEST


def joined_along(tiles, dim):
    tiles = jnp.moveaxis(tiles, 0, dim)
    lengths = tiles.shape
    return tiles.reshape(*lengths[:dim], lengths[dim] * lengths[dim + 1], *lengths[dim + 2 :])


def from_everyone(x, axis):
    peers = lax.axis_size(axis)
    return lax.all_to_all(jnp.broadcast_to(x[None], (peers, *x.shape)), axis, 0, 0, tiled=True)


def collect(x, axis, dim):
    return joined_along(from_everyone(x, axis), dim)


def replay(state_c, state_n, state_m, keys_in, values_in, gates_in, accepted):
    proposals = keys_in.shape[2]
    scaled = keys_in.astype(jnp.float32) * keys_in.shape[3] ** (-0.5)
    values_f = values_in.astype(jnp.float32)
    igates = gates_in[:, :, 0, :]
    forget = jax.nn.log_sigmoid(gates_in[:, :, 1, :])
    position = jnp.arange(proposals, dtype=jnp.int32)
    within = position[None, None, :] < accepted[:, None, None]
    masked = jnp.where(within, forget, 0.0)
    summed = jnp.sum(masked, axis=-1)
    log_weight = jnp.where(
        within, summed[..., None] - jnp.cumsum(masked, axis=-1) + igates, -jnp.inf
    )
    carried_m = jnp.maximum(summed + state_m, jnp.max(log_weight, axis=-1))
    shrink = jnp.exp(summed + state_m - carried_m)
    weights = jnp.exp(log_weight - carried_m[..., None])
    carried_c = shrink[..., None, None] * state_c + jnp.einsum(
        "bhs,bhsv,bhsd->bhvd", weights, values_f, scaled, precision=HIGHEST
    )
    carried_n = shrink[..., None] * state_n + jnp.einsum(
        "bhs,bhsd->bhd", weights, scaled, precision=HIGHEST
    )
    return (carried_c, carried_n, carried_m)


def cell_block(state_c, state_n, state_m, queries, scaled, values_f, igates, forget):
    proposals = queries.shape[2]
    cumul = jnp.cumsum(forget, axis=-1)
    causal = jnp.tril(jnp.ones((proposals, proposals), dtype=bool))
    log_decay = jnp.where(
        causal, cumul[..., :, None] - cumul[..., None, :] + igates[..., None, :], -jnp.inf
    )
    carried = cumul + state_m[..., None]
    stable = jnp.maximum(carried, jnp.max(log_decay, axis=-1))
    scores = jnp.einsum("bhtd,bhsd->bhts", queries, scaled, precision=HIGHEST) * jnp.exp(
        log_decay - stable[..., None]
    )
    weight_state = jnp.exp(carried - stable)
    numer = weight_state[..., None] * jnp.einsum(
        "bhvd,bhtd->bhtv", state_c, queries, precision=HIGHEST
    )
    numer = numer + jnp.einsum("bhts,bhsv->bhtv", scores, values_f, precision=HIGHEST)
    denom = weight_state * jnp.einsum(
        "bhd,bhtd->bht", state_n, queries, precision=HIGHEST
    ) + jnp.sum(scores, axis=-1)
    return numer / jnp.maximum(jnp.abs(denom), jnp.exp(-stable))[..., None]


def gate_heads(hidden, gain, outgate):
    heads_count = hidden.shape[1]
    head_size = hidden.shape[3]
    normed = hidden * lax.rsqrt(jnp.mean(hidden * hidden, axis=-1, keepdims=True) + EPSILON)
    normed = normed * gain.astype(jnp.float32).reshape(heads_count, head_size)[None, :, None, :]
    rows_out = jnp.transpose(normed, (0, 2, 1, 3)).reshape(outgate.shape)
    return (rows_out * jax.nn.sigmoid(outgate.astype(jnp.float32))).astype(jnp.bfloat16)


def per_device(
    tokens,
    norm_gain,
    query_weight,
    key_weight,
    value_weight,
    outgate_weight,
    gate_weight,
    gate_bias,
    head_gain,
    out_weight,
    state_c,
    state_n,
    state_m,
    prev_keys,
    prev_values,
    prev_gates,
    accepted,
):
    seqs_local, proposals, features = tokens.shape
    heads_local = state_m.shape[1]
    head_size = state_n.shape[2]
    tokens_f = tokens.astype(jnp.float32)
    normed = tokens_f * lax.rsqrt(jnp.mean(tokens_f * tokens_f, axis=-1, keepdims=True) + EPSILON)
    normed = (normed * norm_gain.astype(jnp.float32)).astype(jnp.bfloat16)
    rows_in = normed.reshape(seqs_local * proposals, features)

    def project(matrix):
        return jnp.dot(rows_in, matrix, preferred_element_type=jnp.float32).astype(jnp.bfloat16)

    def by_head(array):
        return array.reshape(seqs_local, proposals, heads_local, head_size).transpose(0, 2, 1, 3)

    queries = project(query_weight)
    keys_new = project(key_weight)
    values_new = project(value_weight)
    outgate = project(outgate_weight)
    all_gates = (
        jnp.dot(rows_in, gate_weight, preferred_element_type=jnp.float32)
        + gate_bias.reshape(-1)[None, :]
    )
    heads_total = gate_weight.shape[1] // 2
    head_offset = lax.axis_index("tp") * heads_local
    igates = lax.dynamic_slice_in_dim(all_gates, head_offset, heads_local, 1)
    fgates = lax.dynamic_slice_in_dim(all_gates, heads_total + head_offset, heads_local, 1)
    igates = igates.reshape(seqs_local, proposals, heads_local).transpose(0, 2, 1)
    fgates = fgates.reshape(seqs_local, proposals, heads_local).transpose(0, 2, 1)
    step_gates = jnp.stack([igates, fgates], axis=2)
    carried_c, carried_n, carried_m = replay(
        state_c, state_n, state_m, prev_keys, prev_values, prev_gates, accepted
    )
    step_keys = by_head(keys_new)
    step_values = by_head(values_new)
    hidden = cell_block(
        carried_c,
        carried_n,
        carried_m,
        by_head(queries).astype(jnp.float32),
        step_keys.astype(jnp.float32) * head_size ** (-0.5),
        step_values.astype(jnp.float32),
        igates,
        jax.nn.log_sigmoid(fgates),
    )
    gated = gate_heads(hidden, head_gain, outgate)
    partial_out = jnp.dot(collect(gated, "kv", 0), out_weight, preferred_element_type=jnp.float32)
    summed = lax.psum(partial_out, "tp")
    mixed = summed.astype(jnp.bfloat16).reshape(-1, proposals, summed.shape[1])
    return (mixed, carried_c, carried_n, carried_m, step_keys, step_values, step_gates)


def solution(mesh):
    in_specs = (
        P("kv", None, None),
        P(),
        P(None, "tp"),
        P(None, "tp"),
        P(None, "tp"),
        P(None, "tp"),
        P(),
        P(),
        P("tp"),
        P("tp", "kv"),
        P("kv", "tp", None, None),
        P("kv", "tp", None),
        P("kv", "tp"),
        P("kv", "tp", None, None),
        P("kv", "tp", None, None),
        P("kv", "tp", None, None),
        P("kv"),
    )
    out_specs = (
        P(None, None, "kv"),
        P("kv", "tp", None, None),
        P("kv", "tp", None),
        P("kv", "tp"),
        P("kv", "tp", None, None),
        P("kv", "tp", None, None),
        P("kv", "tp", None, None),
    )
    return jax.shard_map(
        per_device, mesh=mesh, in_specs=in_specs, out_specs=out_specs, check_vma=False
    )
```

profile of v0, /device:TPU:0, one launch (start us, length us, event | category | flops | bytes accessed | tf_op | source)
XLA Modules:
  0.0 114.7 jit_solution(9230726068473415681)
XLA Ops:
  0.6 0.0 copy-start
  0.7 0.8 add.110
  1.5 0.7 iota_compare_fusion
  2.2 0.7 bitcast_convert_fusion
  2.9 0.8 copy.77
  3.6 1.4 %fusion.7 = f32[16,4]{1,0:T(8,128)S(1)} fusion(bf16[16,4,4096]{2,1,0:T(4,128)(2,1)} %param.17), kind=kLoop, calls=%fused_computation.16 | loop fusion | flops 786368 | bytes 524544 | tf_op jit(solution)/shard_map/reduce_sum | solution.py:105
  5.0 0.7 convert_element_type.41
  5.7 0.7 fusion.41
  6.5 0.1 copy.93
  6.6 0.1 copy.76
  6.7 1.4 %fusion.9 = bf16[16,4,4096]{2,1,0:T(4,128)(2,1)S(1)} fusion(bf16[16,4,4096]{2,1,0:T(4,128)(2,1)} %param.17, f32[4096]{0:T(1024)S(1)} %convert_element_type.41, f32[16,4]{1,0:T(8,128)S(1)} %add_rsqrt_fusion), kind=kLoop, calls=%fused_computation.18 | loop fusion | flops 1048576 | bytes 1065216 | tf_op jit(solution)/shard_map/convert_element_type | solution.py:106
  8.1 0.1 reshape.103
  8.2 0.0 copy-done
  8.2 0.3 convolution_add_fusion
  8.5 0.1 reshape.104
  8.6 0.1 reshape.105
  8.7 0.1 fusion.24
  8.8 0.1 fusion.39
  8.9 2.8 %reduce_window_sum.18 = f32[16,4,4]{2,1,0:T(4,128)S(1)} reduce-window(f32[16,4,4]{2,1,0:T(4,128)S(1)} %get-tuple-element.26, f32[]{:T(128)} %constant.13.clone.1), window={size=1x1x4 pad=0_0x0_0x3_0}, to_apply=%region_3.4 | reduce-window | flops 768 | bytes 2052 | tf_op jit(solution)/shard_map/jit(cumsum)/reduce_window_sum | solution.py:36
  11.7 2.7 %reduce_window_sum.17 = f32[16,4,4]{2,1,0:T(4,128)S(1)} reduce-window(f32[16,4,4]{2,1,0:T(4,128)S(1)} %fusion.24, f32[]{:T(128)} %constant.13.clone.1), window={size=1x1x4 pad=0_0x0_0x3_0}, to_apply=%region_1.2 | reduce-window | flops 768 | bytes 2052 | tf_op jit(solution)/shard_map/jit(cumsum)/reduce_window_sum | solution.py:52
  14.4 3.0 %convolution_convert_fusion.1 = bf16[64,512]{1,0:T(8,128)(2,1)S(1)} fusion(bf16[64,4096]{1,0:T(8,128)(2,1)S(1)} %reshape.103, bf16[4096,512]{1,0:T(8,128)(2,1)} %param.21), kind=kOutput, calls=%fused_computation.12 | convolution fusion | flops 268468224 | bytes 4784128 | tf_op jit(solution)/shard_map/dot_general | solution.py:110
  17.5 0.0 copy-start.4
  17.5 3.1 %convolution_convert_fusion.2 = bf16[64,512]{1,0:T(8,128)(2,1)S(1)} fusion(bf16[64,4096]{1,0:T(8,128)(2,1)S(1)} %reshape.103, bf16[4096,512]{1,0:T(8,128)(2,1)} %param.20), kind=kOutput, calls=%fused_computation.13 | convolution fusion | flops 268468224 | bytes 4784128 | tf_op jit(solution)/shard_map/dot_general | solution.py:110
  20.6 0.0 copy-start.8
  20.6 0.0 copy-start.5
  20.6 3.1 %convolution_convert_fusion.3 = bf16[64,512]{1,0:T(8,128)(2,1)S(1)} fusion(bf16[64,4096]{1,0:T(8,128)(2,1)S(1)} %reshape.103, bf16[4096,512]{1,0:T(8,128)(2,1)} %param.19), kind=kOutput, calls=%fused_computation.14 | convolution fusion | flops 268468224 | bytes 4784128 | tf_op jit(solution)/shard_map/dot_general | solution.py:110
  23.7 0.2 fusion.38
  23.9 0.2 fusion.16
  24.1 0.1 subtract_exponential_fusion.1
  24.2 0.0 copy-done.4
  24.2 0.6 fusion.13
  24.8 0.1 copy_bitcast_fusion
  24.9 0.0 copy-start.7
  24.9 0.0 copy-start.6
  24.9 0.0 copy-done.8
  24.9 0.1 multiply_add_fusion.1
  25.0 0.0 copy-start.9
  25.0 0.4 fusion.22
  25.4 0.5 fusion.42
  25.8 0.0 copy-done.9
  25.8 0.1 exponential_maximum_fusion
  25.9 0.1 fusion.29
  26.0 0.0 copy-done.5
  26.0 9.1 %multiply_add_fusion = f32[16,4,128,128]{3,2,1,0:T(8,128)S(1)} fusion(f32[16,4,128,128]{3,2,1,0:T(8,128)} %param.27, f32[16,4]{1,0:T(8,128)S(1)} %get-tuple-element.23, bf16[16,4,4,128]{3,2,1,0:T(4,128)(2,1)S(1)} %copy-done.4, bf16[16,4,4,128]{3,2,1,0:T(4,128)(2,1)S(1)} %copy-done.5, f32[16,4,4]{2,1,0:T(4,128)S(1)} %get-tuple-element.33), kind=kOutput, calls=%fused_computation | convolution fusion | flops 52559872 | bytes 8520960 | tf_op jit(solution)/shard_map/bhs,bhsv,bhsd->bhvd/dot_general | solution.py:41
  35.1 0.0 copy-done.7
  35.2 0.0 copy-start.1
  35.2 0.0 copy-start.2
  35.2 3.3 %fusion.23 = f32[16,4,4,128]{3,2,1,0:T(4,128)S(1)} fusion(f32[16,4,128,128]{3,2,1,0:T(8,128)S(1)} %multiply_add_fusion, bf16[16,4,4,128]{3,2,1,0:T(4,128)(2,1)S(1)} %reshape.106), kind=kOutput, calls=%fused_computation.43 | convolution fusion | flops 50331648 | bytes 4390912 | tf_op jit(solution)/shard_map/bhvd,bhtd->bhtv/dot_general | solution.py:63
  38.5 0.0 copy-done.6
  38.5 0.6 fusion.17
  39.2 0.3 multiply_multiply_fusion
  39.5 0.0 copy-done.2
  39.5 0.9 fusion.6
  40.4 0.0 copy-done.1
  40.4 0.0 copy-start.3
  40.4 1.6 %broadcast_in_dim.52 = bf16[32,64,512]{2,1,0:T(8,128)(2,1)} broadcast(bf16[64,512]{1,0:T(8,128)(2,1)S(1)} %fusion.6), dimensions={1,2} | broadcast | bytes 2162688 | tf_op jit(solution)/shard_map/broadcast_in_dim | solution.py:18
  42.0 8.4 %all-to-all-start = ((bf16[32,64,512]{2,1,0:T(8,128)(2,1)}), bf16[32,64,512]{2,1,0:T(8,128)(2,1)S(1)}, u32[]{:S(2)}, u32[]{:S(2)}) async-start(bf16[32,64,512]{2,1,0:T(8,128)(2,1)} %broadcast_in_dim.52), calls=%async_computation | async-start | bytes 4194304 | tf_op jit(solution)/shard_map/all_to_all | solution.py:18
  50.4 0.7 copy.87
  51.1 0.1 copy.85
  51.2 0.1 copy.86
  51.3 0.6 pad_maximum_fusion
  51.9 28.6 %all-to-all-done = bf16[32,64,512]{2,1,0:T(8,128)(2,1)S(1)} async-done(((bf16[32,64,512]{2,1,0:T(8,128)(2,1)}), bf16[32,64,512]{2,1,0:T(8,128)(2,1)S(1)}, u32[]{:S(2)}, u32[]{:S(2)}) %all-to-all-start) | async-done | bytes 2097184 | tf_op jit(solution)/shard_map/all_to_all | solution.py:18
  80.5 0.7 fusion.43
  81.2 33.5 %all-reduce.1 = bf16[2048,128]{1,0:T(8,128)(2,1)} all-reduce(f32[2048,128]{1,0:T(8,128)S(1)} %fusion.43), channel_id=1, replica_groups=mesh['kv'=32,'tp'=4] {'tp'}, use_global_device_ids=true, to_apply=%region_8.9 | all-reduce | flops 262144 | bytes 1572864 | tf_op jit(solution)/shard_map/psum | solution.py:147
  (12 shorter events, 0.2 us)
Async XLA Ops:
  0.6 7.6 %copy-start = (bf16[4096,32]{0,1:T(8,128)(2,1)S(1)}, bf16[4096,32]{0,1:T(8,128)(2,1)}, u32[]{:S(2)}) copy-start(bf16[4096,32]{0,1:T(8,128)(2,1)} %param.23) | copy-start | bytes 786436
  17.5 6.7 %copy-start.4 = (bf16[16,4,4,128]{3,2,1,0:T(4,128)(2,1)S(1)}, bf16[16,4,4,128]{3,2,1,0:T(4,128)(2,1)}, u32[]{:S(2)}) copy-start(bf16[16,4,4,128]{3,2,1,0:T(4,128)(2,1)} %param.30) | copy-start | bytes 196612
  20.6 4.3 %copy-start.8 = (f32[16,4,128]{2,1,0:T(4,128)S(1)}, f32[16,4,128]{2,1,0:T(4,128)}, u32[]{:S(2)}) copy-start(f32[16,4,128]{2,1,0:T(4,128)} %param.28) | copy-start | bytes 98308
  20.6 5.4 %copy-start.5 = (bf16[16,4,4,128]{3,2,1,0:T(4,128)(2,1)S(1)}, bf16[16,4,4,128]{3,2,1,0:T(4,128)(2,1)}, u32[]{:S(2)}) copy-start(bf16[16,4,4,128]{3,2,1,0:T(4,128)(2,1)} %param.31) | copy-start | bytes 196612
  24.9 10.3 %copy-start.7 = (bf16[16,4,4,128]{3,2,1,0:T(4,128)(2,1)}, bf16[16,4,4,128]{3,2,1,0:T(4,128)(2,1)S(1)}, u32[]{:S(2)}) copy-start(bf16[16,4,4,128]{3,2,1,0:T(4,128)(2,1)S(1)} %get-tuple-element.40) | copy-start | bytes 196612
  24.9 13.7 %copy-start.6 = (bf16[16,4,4,128]{3,2,1,0:T(4,128)(2,1)}, bf16[16,4,4,128]{3,2,1,0:T(4,128)(2,1)S(1)}, u32[]{:S(2)}) copy-start(bf16[16,4,4,128]{3,2,1,0:T(4,128)(2,1)S(1)} %get-tuple-element.39) | copy-start | bytes 196612
  25.0 0.8 copy-start.9
  35.2 5.2 %copy-start.1 = (f32[16,4,128,128]{3,2,1,0:T(8,128)}, f32[16,4,128,128]{3,2,1,0:T(8,128)S(1)}, u32[]{:S(2)}) copy-start(f32[16,4,128,128]{3,2,1,0:T(8,128)S(1)} %multiply_add_fusion) | copy-start | bytes 12582916
  35.2 4.3 %copy-start.2 = (bf16[4096,512]{1,0:T(8,128)(2,1)S(1)}, bf16[4096,512]{1,0:T(8,128)(2,1)}, u32[]{:S(2)}) copy-start(bf16[4096,512]{1,0:T(8,128)(2,1)} %param.22) | copy-start | bytes 12582916
  40.4 40.1 %copy-start.3 = (bf16[512,128]{1,0:T(8,128)(2,1)S(1)}, bf16[512,128]{1,0:T(8,128)(2,1)}, u32[]{:S(2)}) copy-start(bf16[512,128]{1,0:T(8,128)(2,1)} %param.26) | copy-start | bytes 393220
  42.0 38.5 %all-to-all-start = ((bf16[32,64,512]{2,1,0:T(8,128)(2,1)}), bf16[32,64,512]{2,1,0:T(8,128)(2,1)S(1)}, u32[]{:S(2)}, u32[]{:S(2)}) async-start(bf16[32,64,512]{2,1,0:T(8,128)(2,1)} %broadcast_in_dim.52), calls=%async_computation | async-start | bytes 4194304 | tf_op jit(solution)/shard_map/all_to_all | solution.py:18
where the time goes:
time: 115 us
  blocking collectives  33.5 us (29%)
  waiting for transfers between devices  28.6 us (25%)
  matrix products  25.4 us (22%)
  other arithmetic  12.3 us (11%)
  starting transfers between devices  8.44 us (7%)
  local copies, waits for them, and re-layouts  5.47 us (5%)
    psum x1, blocking collectives, per_device(): summed = lax.psum(partial_out, 'tp')  33.5 us
    all_to_all x1, waiting for transfers between devices, from_everyone(): lax.all_to_all(jnp.broadcast_to(x[None], (peers, *x.shape)), axis, 0, 0,...  28.6 us
    dot_general x4, matrix products, project(): jnp.dot(rows_in, matrix, preferred_element_type=jnp.float32)  9.99 us
    dot_general x1, matrix products, replay(): jnp.einsum('bhs,bhsv,bhsd->bhvd', weights, values_f, scaled, precision=HI...  9.09 us
    all_to_all x1, starting transfers between devices, from_everyone(): lax.all_to_all(jnp.broadcast_to(x[None], (peers, *x.shape)), axis, 0, 0,...  8.44 us
    dot_general x1, matrix products, cell_block(): jnp.einsum('bhvd,bhtd->bhtv', state_c, queries, precision=HIGHEST)  3.35 us
    another operation x1, other arithmetic, replay(): jnp.cumsum(masked, axis=-1)  2.76 us
    another operation x1, other arithmetic, cell_block(): cumul = jnp.cumsum(forget, axis=-1)  2.75 us
  transfers between devices with their start and end apart: 1, of which 1 were waited for; matrix products, arithmetic and copies ran while one was open for 1% of the time, Pallas kernels for 0%

commit v1 on v0

--- a/solution.py
+++ b/solution.py
@@ -7,19 +7,50 @@
 HIGHEST = lax.Precision.HIGHEST
 
 
-def joined_along(tiles, dim):
-    tiles = jnp.moveaxis(tiles, 0, dim)
-    lengths = tiles.shape
-    return tiles.reshape(*lengths[:dim], lengths[dim] * lengths[dim + 1], *lengths[dim + 2 :])
-
-
-def from_everyone(x, axis):
-    peers = lax.axis_size(axis)
-    return lax.all_to_all(jnp.broadcast_to(x[None], (peers, *x.shape)), axis, 0, 0, tiled=True)
-
-
-def collect(x, axis, dim):
-    return joined_along(from_everyone(x, axis), dim)
+def ring(count, step):
+    return [(i, (i + step) % count) for i in range(count)]
+
+
+def cores_apart(kv, tp):
+    return [[(chip * 2 + core) * tp + x for chip in range(kv // 2) for x in range(tp)] for core in (0, 1)]
+
+
+def gather_weight(weight):
+    tp = lax.axis_size("tp")
+    me = lax.axis_index("tp")
+    full = jnp.zeros((tp, *weight.shape), weight.dtype)
+    full = lax.dynamic_update_index_in_dim(full, weight, me, 0)
+    for step in range(1, tp):
+        part = lax.ppermute(weight, "tp", ring(tp, step))
+        full = lax.dynamic_update_index_in_dim(full, part, lax.rem(me - step + tp, tp), 0)
+    return full
+
+
+def project_out(gated, weight):
+    kv, tp = lax.axis_size("kv"), lax.axis_size("tp")
+    chips = kv // 2
+    rows = gated.shape[0] // tp
+    sent = jnp.broadcast_to(gated.reshape(1, tp, rows, -1), (chips, tp, rows, gated.shape[1]))
+    sent = sent.reshape(chips * tp, rows, -1)
+    own = lax.all_to_all(
+        sent, ("kv", "tp"), 0, 0, tiled=True, axis_index_groups=cores_apart(kv, tp)
+    )
+    swap = [(i, i ^ 1) for i in range(kv)]
+    other = lax.ppermute(own, "kv", swap)
+
+    def times(part):
+        part = part.reshape(chips, tp, rows, -1)
+        return jnp.einsum(
+            "zxrk,xkn->zrn", part, weight, preferred_element_type=jnp.float32
+        ).astype(jnp.bfloat16)
+
+    first, second = times(own), times(other)
+    core = lax.rem(lax.axis_index("kv"), 2)
+    even = jnp.where(core == 0, first, second)
+    odd = jnp.where(core == 0, second, first)
+    mine = jnp.stack([even, odd], axis=1)
+    everyone = lax.all_gather(mine, "tp", axis=0)
+    return everyone.transpose(1, 2, 0, 3, 4).reshape(-1, weight.shape[2])
 
 
 def replay(state_c, state_n, state_m, keys_in, values_in, gates_in, accepted):
@@ -143,9 +174,8 @@
         jax.nn.log_sigmoid(fgates),
     )
     gated = gate_heads(hidden, head_gain, outgate)
-    partial_out = jnp.dot(collect(gated, "kv", 0), out_weight, preferred_element_type=jnp.float32)
-    summed = lax.psum(partial_out, "tp")
-    mixed = summed.astype(jnp.bfloat16).reshape(-1, proposals, summed.shape[1])
+    mixed = project_out(gated, gather_weight(out_weight))
+    mixed = mixed.reshape(-1, proposals, mixed.shape[1])
     return (mixed, carried_c, carried_n, carried_m, step_keys, step_values, step_gates)
 
 

time: 115 us -> 96.3 us (0.84)
  waiting for transfers between devices: 28.6 us -> 5.16 us
  blocking collectives: 33.5 us -> 43.2 us
  starting transfers between devices: 8.44 us -> 3.3 us
    psum x1 -> x0, blocking collectives: 33.5 us -> none  [per_device(): summed = lax.psum(partial_out, 'tp')]
    all_to_all x0 -> x1, blocking collectives: none -> 30.4 us  [project_out(): lax.all_to_all(sent, ('kv', 'tp'), 0, 0, tiled=True, axis_index_groups=co...]
    all_to_all x1 -> x0, waiting for transfers between devices: 28.6 us -> none  [from_everyone(): lax.all_to_all(jnp.broadcast_to(x[None], (peers, *x.shape)), axis, 0, 0,...]
    all_gather x0 -> x1, blocking collectives: none -> 12.8 us  [project_out(): everyone = lax.all_gather(mine, 'tp', axis=0)]
    all_to_all x1 -> x0, starting transfers between devices: 8.44 us -> none  [from_everyone(): lax.all_to_all(jnp.broadcast_to(x[None], (peers, *x.shape)), axis, 0, 0,...]
    ppermute x0 -> x4, waiting for transfers between devices: none -> 5.16 us  [the longest x3 5.15 us: gather_weight(): part = lax.ppermute(weight, 'tp', ring(tp, step))]
    ppermute x0 -> x4, starting transfers between devices: none -> 3.3 us  [the longest x3 3.3 us: gather_weight(): part = lax.ppermute(weight, 'tp', ring(tp, step))]
    broadcast_in_dim x1 -> x2, local copies, waits for them, and re-layouts: 1.59 us -> 0.19 us  [the longest x1 0.12 us: project_out(): jnp.broadcast_to(gated.reshape(1, tp, rows, -1), (chips, tp, rows, gated....]
  transfers between devices with their start and end apart: 1 -> 4, of which waited for: 1 -> 2; matrix products, arithmetic and copies ran while one was open for 1% -> 2% of each run, Pallas kernels for 0% -> 0%
where the time goes in v1:
time: 96.3 us; the launch traced here: 95.6 us
  blocking collectives  43.2 us (45%)
  matrix products  25.5 us (26%)
  other arithmetic  12.3 us (13%)
  waiting for transfers between devices  5.16 us (5%)
  local copies, waits for them, and re-layouts  5.01 us (5%)
  starting transfers between devices  3.3 us (3%)
  between operations  1.11 us (1%)
    all_to_all x1, blocking collectives, project_out(): lax.all_to_all(sent, ('kv', 'tp'), 0, 0, tiled=True, axis_index_groups=co...  30.4 us
    all_gather x1, blocking collectives, project_out(): everyone = lax.all_gather(mine, 'tp', axis=0)  12.8 us
    dot_general x4, matrix products, project(): jnp.dot(rows_in, matrix, preferred_element_type=jnp.float32)  9.99 us
    dot_general x1, matrix products, replay(): jnp.einsum('bhs,bhsv,bhsd->bhvd', weights, values_f, scaled, precision=HI...  9.09 us
    ppermute x3, waiting for transfers between devices, gather_weight(): part = lax.ppermute(weight, 'tp', ring(tp, step))  5.15 us
    dot_general x1, matrix products, cell_block(): jnp.einsum('bhvd,bhtd->bhtv', state_c, queries, precision=HIGHEST)  3.35 us
    ppermute x3, starting transfers between devices, gather_weight(): part = lax.ppermute(weight, 'tp', ring(tp, step))  3.3 us
    another operation x1, other arithmetic, replay(): jnp.cumsum(masked, axis=-1)  2.76 us
  transfers between devices with their start and end apart: 4, of which 2 were waited for; matrix products, arithmetic and copies ran while one was open for 2% of the time, Pallas kernels for 0%

profile of v1, /device:TPU:0, one launch (start us, length us, event | category | flops | bytes accessed | tf_op | source)
XLA Modules:
  0.0 95.6 jit_solution(14246280771062492849)
XLA Ops:
  0.6 0.0 copy-start
  0.7 0.8 add.139
  1.5 0.7 iota_compare_fusion
  2.2 0.7 bitcast_convert_fusion
  2.9 0.8 copy.80
  3.6 1.4 %fusion.9 = f32[16,4]{1,0:T(8,128)S(1)} fusion(bf16[16,4,4096]{2,1,0:T(4,128)(2,1)} %param.17), kind=kLoop, calls=%fused_computation.20 | loop fusion | flops 786368 | bytes 524544 | tf_op jit(solution)/shard_map/reduce_sum | solution.py:136
  5.0 0.7 convert_element_type.44
  5.8 0.7 fusion.45
  6.5 0.1 copy.99
  6.6 0.1 copy.79
  6.7 1.4 %fusion.11 = bf16[16,4,4096]{2,1,0:T(4,128)(2,1)S(1)} fusion(bf16[16,4,4096]{2,1,0:T(4,128)(2,1)} %param.17, f32[4096]{0:T(1024)S(1)} %convert_element_type.44, f32[16,4]{1,0:T(8,128)S(1)} %add_rsqrt_fusion), kind=kLoop, calls=%fused_computation.22 | loop fusion | flops 1048576 | bytes 1065216 | tf_op jit(solution)/shard_map/convert_element_type | solution.py:137
  8.1 0.1 reshape.107
  8.2 0.3 convolution_add_fusion
  8.5 0.1 reshape.108
  8.6 0.1 reshape.109
  8.7 0.1 fusion.28
  8.8 0.1 fusion.43
  8.9 2.8 %reduce_window_sum.18 = f32[16,4,4]{2,1,0:T(4,128)S(1)} reduce-window(f32[16,4,4]{2,1,0:T(4,128)S(1)} %get-tuple-element.26, f32[]{:T(128)} %constant.64.clone.1), window={size=1x1x4 pad=0_0x0_0x3_0}, to_apply=%region_3.4 | reduce-window | flops 768 | bytes 2052 | tf_op jit(solution)/shard_map/jit(cumsum)/reduce_window_sum | solution.py:67
  11.7 2.7 %reduce_window_sum.17 = f32[16,4,4]{2,1,0:T(4,128)S(1)} reduce-window(f32[16,4,4]{2,1,0:T(4,128)S(1)} %fusion.28, f32[]{:T(128)} %constant.64.clone.1), window={size=1x1x4 pad=0_0x0_0x3_0}, to_apply=%region_1.2 | reduce-window | flops 768 | bytes 2052 | tf_op jit(solution)/shard_map/jit(cumsum)/reduce_window_sum | solution.py:83
  14.4 3.0 %convolution_convert_fusion.1 = bf16[64,512]{1,0:T(8,128)(2,1)S(1)} fusion(bf16[64,4096]{1,0:T(8,128)(2,1)S(1)} %reshape.107, bf16[4096,512]{1,0:T(8,128)(2,1)} %param.21), kind=kOutput, calls=%fused_computation.16 | convolution fusion | flops 268468224 | bytes 4784128 | tf_op jit(solution)/shard_map/dot_general | solution.py:141
  17.5 0.0 copy-start.4
  17.5 3.1 %convolution_convert_fusion.2 = bf16[64,512]{1,0:T(8,128)(2,1)S(1)} fusion(bf16[64,4096]{1,0:T(8,128)(2,1)S(1)} %reshape.107, bf16[4096,512]{1,0:T(8,128)(2,1)} %param.20), kind=kOutput, calls=%fused_computation.17 | convolution fusion | flops 268468224 | bytes 4784128 | tf_op jit(solution)/shard_map/dot_general | solution.py:141
  20.6 0.0 copy-start.8
  20.6 0.0 copy-start.5
  20.6 3.1 %convolution_convert_fusion.3 = bf16[64,512]{1,0:T(8,128)(2,1)S(1)} fusion(bf16[64,4096]{1,0:T(8,128)(2,1)S(1)} %reshape.107, bf16[4096,512]{1,0:T(8,128)(2,1)} %param.19), kind=kOutput, calls=%fused_computation.18 | convolution fusion | flops 268468224 | bytes 4784128 | tf_op jit(solution)/shard_map/dot_general | solution.py:141
  23.7 0.2 fusion.42
  23.9 0.2 fusion.20
  24.1 0.1 subtract_exponential_fusion.1
  24.2 0.6 fusion.17
  24.8 0.1 copy_bitcast_fusion
  24.9 0.0 copy-start.7
  24.9 0.0 copy-start.6
  24.9 0.1 multiply_add_fusion.1
  25.0 0.0 copy-start.9
  25.0 0.3 fusion.26
  25.3 0.5 fusion.46
  25.8 0.1 exponential_maximum_fusion
  25.9 0.1 fusion.33
  26.0 9.1 %multiply_add_fusion = f32[16,4,128,128]{3,2,1,0:T(8,128)S(1)} fusion(f32[16,4,128,128]{3,2,1,0:T(8,128)} %param.27, f32[16,4]{1,0:T(8,128)S(1)} %get-tuple-element.23, bf16[16,4,4,128]{3,2,1,0:T(4,128)(2,1)S(1)} %copy-done.4, bf16[16,4,4,128]{3,2,1,0:T(4,128)(2,1)S(1)} %copy-done.5, f32[16,4,4]{2,1,0:T(4,128)S(1)} %get-tuple-element.35), kind=kOutput, calls=%fused_computation | convolution fusion | flops 52559872 | bytes 8520960 | tf_op jit(solution)/shard_map/bhs,bhsv,bhsd->bhvd/dot_general | solution.py:72
  35.1 0.0 copy-start.1
  35.2 0.0 copy-start.2
  35.2 3.3 %fusion.27 = f32[16,4,4,128]{3,2,1,0:T(4,128)S(1)} fusion(f32[16,4,128,128]{3,2,1,0:T(8,128)S(1)} %multiply_add_fusion, bf16[16,4,4,128]{3,2,1,0:T(4,128)(2,1)S(1)} %reshape.110), kind=kOutput, calls=%fused_computation.56 | convolution fusion | flops 50331648 | bytes 4390912 | tf_op jit(solution)/shard_map/bhvd,bhtd->bhtv/dot_general | solution.py:94
  38.5 0.6 fusion.21
  39.2 0.3 multiply_multiply_fusion
  39.4 0.0 copy-start.3
  39.5 0.9 fusion.8
  40.4 0.1 broadcast_in_dim.70
  40.5 30.4 %all_to_all.5 = bf16[64,16,512]{2,1,0:T(8,128)(2,1)S(1)} all-to-all(bf16[64,16,512]{2,1,0:T(8,128)(2,1)S(1)} %bitcast.166), channel_id=1, replica_groups={{0,1,2,3,8,9,10,11,16,17,18,19,24,25,26,27,32,33,34,35,40,41,42,43,48,4..., dimensions={0} | all-to-all | bytes 2097152 | tf_op jit(solution)/shard_map/all_to_all | solution.py:35
  70.9 0.0 collective-permute-start.3
  70.9 0.6 collective-permute-start
  71.5 2.7 %collective-permute-start.2 = (bf16[512,128]{1,0:T(8,128)(2,1)S(1)}, bf16[512,128]{1,0:T(8,128)(2,1)S(1)}, u32[]{:S(2)}, u32[]{:S(2)}) collective-permute-start(bf16[512,128]{1,0:T(8,128)(2,1)S(1)} %copy-done.3), channel_id=1, source_target_pairs={{0,3},{1,0},{2,1},{3,2},{4,7},{5,4},{6,5},{7,6},{8,11},{9,8},{10,9... | collective-permute-start | bytes 393224 | tf_op jit(solution)/shard_map/ppermute | solution.py:24
  74.2 0.1 collective-permute-start.1
  74.2 0.1 broadcast_in_dim.71
  74.4 0.7 copy.91
  75.0 0.1 copy.89
  75.1 0.1 copy.90
  75.2 0.6 pad_maximum_fusion.1
  75.8 2.2 %collective-permute-done = bf16[512,128]{1,0:T(8,128)(2,1)S(1)} collective-permute-done((bf16[512,128]{1,0:T(8,128)(2,1)S(1)}, bf16[512,128]{1,0:T(8,128)(2,1)S(1)}, u32[]{:S(2)}, u32[]{:S(2)}) %collective-permute-start) | collective-permute-done | bytes 131104 | tf_op jit(solution)/shard_map/ppermute | solution.py:24
  78.1 2.9 %collective-permute-done.1 = bf16[512,128]{1,0:T(8,128)(2,1)S(1)} collective-permute-done((bf16[512,128]{1,0:T(8,128)(2,1)S(1)}, bf16[512,128]{1,0:T(8,128)(2,1)S(1)}, u32[]{:S(2)}, u32[]{:S(2)}) %collective-permute-start.1) | collective-permute-done | bytes 131104 | tf_op jit(solution)/shard_map/ppermute | solution.py:24
  81.0 0.0 collective-permute-done.2
  81.1 0.4 fusion.1
  81.5 0.4 select_bitcast_fusion.1
  82.0 12.8 %all-gather = bf16[64,2,16,128]{3,2,0,1:T(8,128)(2,1)S(1)} all-gather(bf16[16,2,16,128]{3,2,0,1:T(8,128)(2,1)S(1)} %pad_maximum_fusion), channel_id=2, replica_groups=mesh['kv'=32,'tp'=4] {'tp'}, dimensions={0}, use_global_device_ids=true | all-gather | bytes 655360 | tf_op jit(solution)/shard_map/all_gather | solution.py:52
  94.8 0.9 copy.88
  (27 shorter events, 0.3 us)
Async XLA Ops:
  0.6 7.6 %copy-start = (bf16[4096,32]{0,1:T(8,128)(2,1)S(1)}, bf16[4096,32]{0,1:T(8,128)(2,1)}, u32[]{:S(2)}) copy-start(bf16[4096,32]{0,1:T(8,128)(2,1)} %param.23) | copy-start | bytes 786436
  17.5 6.7 %copy-start.4 = (bf16[16,4,4,128]{3,2,1,0:T(4,128)(2,1)S(1)}, bf16[16,4,4,128]{3,2,1,0:T(4,128)(2,1)}, u32[]{:S(2)}) copy-start(bf16[16,4,4,128]{3,2,1,0:T(4,128)(2,1)} %param.30) | copy-start | bytes 196612
  20.6 4.3 %copy-start.8 = (f32[16,4,128]{2,1,0:T(4,128)S(1)}, f32[16,4,128]{2,1,0:T(4,128)}, u32[]{:S(2)}) copy-start(f32[16,4,128]{2,1,0:T(4,128)} %param.28) | copy-start | bytes 98308
  20.6 5.4 %copy-start.5 = (bf16[16,4,4,128]{3,2,1,0:T(4,128)(2,1)S(1)}, bf16[16,4,4,128]{3,2,1,0:T(4,128)(2,1)}, u32[]{:S(2)}) copy-start(bf16[16,4,4,128]{3,2,1,0:T(4,128)(2,1)} %param.31) | copy-start | bytes 196612
  24.9 10.3 %copy-start.7 = (bf16[16,4,4,128]{3,2,1,0:T(4,128)(2,1)}, bf16[16,4,4,128]{3,2,1,0:T(4,128)(2,1)S(1)}, u32[]{:S(2)}) copy-start(bf16[16,4,4,128]{3,2,1,0:T(4,128)(2,1)S(1)} %get-tuple-element.42) | copy-start | bytes 196612
  24.9 13.7 %copy-start.6 = (bf16[16,4,4,128]{3,2,1,0:T(4,128)(2,1)}, bf16[16,4,4,128]{3,2,1,0:T(4,128)(2,1)S(1)}, u32[]{:S(2)}) copy-start(bf16[16,4,4,128]{3,2,1,0:T(4,128)(2,1)S(1)} %get-tuple-element.41) | copy-start | bytes 196612
  25.0 10.2 %copy-start.9 = (f32[16,4,128]{2,1,0:T(4,128)}, f32[16,4,128]{2,1,0:T(4,128)S(1)}, u32[]{:S(2)}) copy-start(f32[16,4,128]{2,1,0:T(4,128)S(1)} %multiply_add_fusion.1) | copy-start | bytes 98308
  35.1 5.2 %copy-start.1 = (f32[16,4,128,128]{3,2,1,0:T(8,128)}, f32[16,4,128,128]{3,2,1,0:T(8,128)S(1)}, u32[]{:S(2)}) copy-start(f32[16,4,128,128]{3,2,1,0:T(8,128)S(1)} %multiply_add_fusion) | copy-start | bytes 12582916
  35.2 4.3 %copy-start.2 = (bf16[4096,512]{1,0:T(8,128)(2,1)S(1)}, bf16[4096,512]{1,0:T(8,128)(2,1)}, u32[]{:S(2)}) copy-start(bf16[4096,512]{1,0:T(8,128)(2,1)} %param.22) | copy-start | bytes 12582916
  39.4 31.5 %copy-start.3 = (bf16[512,128]{1,0:T(8,128)(2,1)S(1)}, bf16[512,128]{1,0:T(8,128)(2,1)}, u32[]{:S(2)}) copy-start(bf16[512,128]{1,0:T(8,128)(2,1)} %param.26) | copy-start | bytes 393220
  70.9 10.2 %collective-permute-start.3 = (bf16[64,16,512]{2,1,0:T(8,128)(2,1)S(1)}, bf16[64,16,512]{2,1,0:T(8,128)(2,1)S(1)}, u32[]{:S(2)}, u32[]{:S(2)}) collective-permute-start(bf16[64,16,512]{2,1,0:T(8,128)(2,1)S(1)} %all_to_all.5), channel_id=1, source_target_pairs={{0,4},{4,0},{8,12},{12,8},{16,20},{20,16},{24,28},{28,24},{32,36},... | collective-permute-start | bytes 3145736 | tf_op jit(solution)/shard_map/ppermute | solution.py:39
  70.9 7.1 %collective-permute-start = (bf16[512,128]{1,0:T(8,128)(2,1)S(1)}, bf16[512,128]{1,0:T(8,128)(2,1)S(1)}, u32[]{:S(2)}, u32[]{:S(2)}) collective-permute-start(bf16[512,128]{1,0:T(8,128)(2,1)S(1)} %copy-done.3), channel_id=1, source_target_pairs={{0,1},{1,2},{2,3},{3,0},{4,5},{5,6},{6,7},{7,4},{8,9},{9,10},{10,1... | collective-permute-start | bytes 393224 | tf_op jit(solution)/shard_map/ppermute | solution.py:24
  71.5 9.5 %collective-permute-start.2 = (bf16[512,128]{1,0:T(8,128)(2,1)S(1)}, bf16[512,128]{1,0:T(8,128)(2,1)S(1)}, u32[]{:S(2)}, u32[]{:S(2)}) collective-permute-start(bf16[512,128]{1,0:T(8,128)(2,1)S(1)} %copy-done.3), channel_id=1, source_target_pairs={{0,3},{1,0},{2,1},{3,2},{4,7},{5,4},{6,5},{7,6},{8,11},{9,8},{10,9... | collective-permute-start | bytes 393224 | tf_op jit(solution)/shard_map/ppermute | solution.py:24
  74.2 6.9 %collective-permute-start.1 = (bf16[512,128]{1,0:T(8,128)(2,1)S(1)}, bf16[512,128]{1,0:T(8,128)(2,1)S(1)}, u32[]{:S(2)}, u32[]{:S(2)}) collective-permute-start(bf16[512,128]{1,0:T(8,128)(2,1)S(1)} %copy-done.3), channel_id=1, source_target_pairs={{0,2},{1,3},{2,0},{3,1},{4,6},{5,7},{6,4},{7,5},{8,10},{9,11},{10,... | collective-permute-start | bytes 393224 | tf_op jit(solution)/shard_map/ppermute | solution.py:24

commit v2 on v0

v2 whole, which is shorter than its diff:
```python
import jax
import jax.numpy as jnp
from jax import lax
from jax.experimental import pallas as pl
from jax.experimental.pallas import tpu as pltpu
from jax.sharding import PartitionSpec as P


EPSILON = 1e-06
HIGHEST = lax.Precision.HIGHEST


def ring(count, step):
    return [(i, (i + step) % count) for i in range(count)]


def swap_cores(x):
    return lax.ppermute(x, "kv", [(i, i ^ 1) for i in range(lax.axis_size("kv"))])


def passed_on(weight):
    tp = lax.axis_size("tp")
    return [weight] + [lax.ppermute(weight, "tp", ring(tp, step)) for step in range(1, tp)]


def mix_kernel(received, *refs):
    weights, out = refs[:-1], refs[-1]
    chips, tp, rows, depth = received.shape
    me = lax.axis_index("tp")
    core = lax.rem(lax.axis_index("kv"), 2)
    total = None
    for step in range(tp):
        source = lax.rem(me - step + tp, tp)
        part = received[:, pl.ds(source, 1)].reshape(chips * rows, depth)
        both = jnp.concatenate([weights[step][...], weights[tp + step][...]], axis=1)
        dot = jnp.dot(part, both, preferred_element_type=jnp.float32)
        total = dot if total is None else total + dot
    mixed = total.astype(jnp.bfloat16)
    columns = mixed.shape[1] // 2
    for x in range(tp):
        out[core, x] = mixed[:, :columns]
        out[1 - core, x] = mixed[:, columns:]


def same_core(kv, tp):
    return [
        [(chip * 2 + core) * tp + x for chip in range(kv // 2) for x in range(tp)]
        for core in (0, 1)
    ]


def same_line(kv, tp):
    return [
        [(chip * 2 + core) * tp + x for core in (0, 1) for x in range(tp)]
        for chip in range(kv // 2)
    ]


def project_out(sent, own_parts):
    kv, tp = lax.axis_size("kv"), lax.axis_size("tp")
    chips = kv // 2
    rows, depth = sent.shape[1] // tp, sent.shape[2]
    other_parts = [swap_cores(part) for part in own_parts]
    received = lax.all_to_all(
        sent.reshape(chips * tp, rows, depth), ("kv", "tp"), 0, 0,
        tiled=True, axis_index_groups=same_core(kv, tp),
    ).reshape(chips, tp, rows, depth)
    columns = own_parts[0].shape[1]
    mixed = pl.pallas_call(
        mix_kernel,
        out_shape=jax.ShapeDtypeStruct((2, tp, chips * rows, columns), jnp.bfloat16),
        compiler_params=pltpu.CompilerParams(vmem_limit_bytes=12 * 1024 * 1024),
        cost_estimate=pl.CostEstimate(
            flops=4 * chips * rows * tp * depth * columns,
            bytes_accessed=3 << 20,
            transcendentals=0,
        ),
    )(received, *own_parts, *other_parts)
    everyone = lax.all_to_all(
        mixed.reshape(2 * tp, chips * rows, columns), ("kv", "tp"), 0, 0,
        tiled=True, axis_index_groups=same_line(kv, tp),
    ).reshape(2, tp, chips, rows, columns)
    return everyone.transpose(2, 0, 1, 3, 4).reshape(-1, columns)


def split(x):
    high = x.astype(jnp.bfloat16)
    return high, (x - high.astype(jnp.float32)).astype(jnp.bfloat16)


def exact_dot(a, b, contract):
    return lax.dot_general(
        a, b, ((contract[:1], contract[1:]), ((), ())),
        precision=HIGHEST, preferred_element_type=jnp.float32,
    )


def dot_nt(a, b):
    return lax.dot_general(
        a, b, (((1,), (1,)), ((), ())), preferred_element_type=jnp.float32
    )


def log_sigmoid(x):
    return jnp.minimum(x, 0.0) - jnp.log1p(jnp.exp(-jnp.abs(x)))


def iota(shape, dim):
    return lax.broadcasted_iota(jnp.int32, shape, dim)


def cell_kernel(
    accepted,
    tokens,
    norm_gain,
    query_weight,
    key_weight,
    value_weight,
    outgate_weight,
    gate_weight,
    gate_bias,
    head_gain,
    state_c,
    state_n,
    state_m,
    prev_keys,
    prev_values,
    prev_gates,
    gated_out,
    carried_c,
    carried_n,
    carried_m,
    step_keys,
    step_values,
    step_gates,
    tokens_v,
    gain_v,
    weights_v,
    gate_weight_v,
    gate_bias_v,
    head_gain_v,
    state_c_v,
    state_n_v,
    state_m_v,
    prev_keys_v,
    prev_values_v,
    prev_gates_v,
    normed_f,
    normed_v,
    recall_v,
    gated_v,
    sems,
    out_sems,
):
    f32, bf16 = jnp.float32, jnp.bfloat16
    seqs, props, width = tokens_v.shape
    heads, _, size, _ = state_c_v.shape
    rows = seqs * props
    heads_total = gate_weight_v.shape[0] // 2
    scale = size ** (-0.5)
    pieces = 4
    depth = width // pieces

    copies = []

    def bring(src, dst):
        copy = pltpu.make_async_copy(src, dst, sems.at[len(copies)])
        copies.append(copy)
        copy.start()
        return copy

    def bring_weight(which, src):
        return [
            bring(src.at[pl.ds(p * depth, depth)], weights_v.at[which, pl.ds(p * depth, depth)])
            for p in range(pieces)
        ]

    early = [bring(tokens, tokens_v), bring(norm_gain, gain_v)]
    gates_in = [bring(gate_weight, gate_weight_v), bring(gate_bias, gate_bias_v)]
    replay_in = [
        bring(state_m, state_m_v),
        bring(prev_gates, prev_gates_v),
        bring(state_n, state_n_v),
        bring(prev_keys, prev_keys_v),
        bring(prev_values, prev_values_v),
        bring(head_gain, head_gain_v),
    ]
    weights_in = [bring_weight(0, query_weight)]
    states_in = [bring(state_c.at[:, h], state_c_v.at[h]) for h in range(heads)]
    weights_in += [
        bring_weight(1, key_weight),
        bring_weight(2, value_weight),
        bring_weight(3, outgate_weight),
    ]

    def arrive(some):
        for copy in some:
            copy.wait()

    row_lane = iota((1, rows), 1)
    prop_lane = row_lane & (props - 1)
    spread = jnp.where(iota((seqs, rows), 0) == (iota((seqs, rows), 1) >> 2), 1.0, 0.0)
    spread_t = jnp.where((iota((rows, seqs), 0) >> 2) == iota((rows, seqs), 1), 1.0, 0.0)
    square = (rows, rows)
    same = (iota(square, 0) >> 2) == (iota(square, 1) >> 2)
    causal = same & (iota(square, 0) >= iota(square, 1))

    arrive(early)
    gain = gain_v[...].astype(f32)
    for b in range(seqs):
        x = tokens_v[b].astype(f32)
        mean = jnp.mean(x * x, axis=-1, keepdims=True)
        normed_f[b * props : (b + 1) * props, :] = x * lax.rsqrt(mean + EPSILON) * gain
    normed_v[...] = normed_f[...].astype(bf16)

    arrive(gates_in)
    bias = jnp.concatenate([gate_bias_v[0:1, :], gate_bias_v[1:2, :]], axis=1)
    gates = dot_nt(normed_v[...], gate_weight_v[...]) + bias
    gates = jnp.concatenate([gates, jnp.zeros((rows, 128 - 2 * heads_total), f32)], axis=1)
    first_head = lax.axis_index("tp") * heads
    gates = pltpu.roll(gates, 128 - first_head, 1)
    forget = log_sigmoid(gates)
    cumul = exact_dot(jnp.where(causal, 1.0, 0.0), forget, (1, 0))
    gates_t = gates.T
    cumul_t = cumul.T
    for t in range(props):
        pick = jnp.where(iota((rows, seqs), 0) == iota((rows, seqs), 1) * props + t, 1.0, 0.0)
        picked = exact_dot(gates_t[: 2 * heads_total], pick, (1, 0))
        for h in range(heads):
            step_gates[h, 0, t : t + 1, :] = picked[h : h + 1, :]
            step_gates[h, 1, t : t + 1, :] = picked[heads_total + h : heads_total + h + 1, :]

    arrive(replay_in)
    seq_lane = iota((1, seqs), 1)
    counts = jnp.zeros((1, seqs), jnp.int32)
    for b in range(seqs):
        counts = jnp.where(seq_lane == b, accepted[b], counts)
    total = jnp.zeros((heads, seqs), f32)
    sums, inputs = [], []
    for s in range(props):
        both = [
            jnp.concatenate([prev_gates_v[h, g, s : s + 1, :] for h in range(heads)], axis=0)
            for g in (0, 1)
        ]
        total = total + jnp.where(counts > s, log_sigmoid(both[1]), 0.0)
        sums.append(total)
        inputs.append(both[0])
    logs = [
        jnp.where(counts > s, total - sums[s] + inputs[s], -jnp.inf) for s in range(props)
    ]
    decayed = total + state_m_v[...]
    stable = decayed
    for s in range(props):
        stable = jnp.maximum(stable, logs[s])
    carried_m[...] = stable
    shrink = jnp.exp(decayed - stable)
    weights = jnp.zeros((heads, rows), f32)
    for s in range(props):
        spaced = exact_dot(jnp.exp(logs[s] - stable), spread, (1, 0))
        weights = weights + jnp.where(prop_lane == s, spaced, 0.0)
    weights = weights * scale
    stable_col = exact_dot(spread_t, stable, (1, 1))
    diagonal = jnp.where(iota((seqs, seqs), 0) == iota((seqs, seqs), 1), 1.0, 0.0)
    shrink_col = exact_dot(diagonal, shrink, (1, 1))

    def project(which):
        acc = None
        for p in range(pieces):
            weights_in[which][p].wait()
            part = jnp.dot(
                normed_v[:, p * depth : (p + 1) * depth],
                weights_v[which, p * depth : (p + 1) * depth, :],
                preferred_element_type=f32,
            )
            acc = part if acc is None else acc + part
        return acc.astype(bf16)

    queries = project(0)
    out_copies = []
    seq_of_lane = (iota((1, 2 * rows), 1) & (rows - 1)) >> 2
    upper = iota((2 * props, size), 0) < props
    recall_norm = []
    for h in range(heads):
        cols = slice(h * size, (h + 1) * size)
        query = queries[:, cols]
        query_f = query.astype(f32)
        keys = prev_keys_v[:, h].astype(f32).reshape(rows, size)
        values = prev_values_v[:, h].astype(f32).reshape(rows, size)
        weight = weights[h : h + 1, :]
        norm = shrink_col[:, h : h + 1] * state_n_v[:, h, :] + exact_dot(
            spread * weight, keys, (1, 0)
        )
        carried_n[:, h, :] = norm
        along = exact_dot(query_f, norm, (1, 1))
        recall_norm.append(jnp.sum(along * spread_t, axis=1, keepdims=True))
        weighted = jnp.concatenate(split(values.T * weight), axis=1)
        key_pair = jnp.concatenate([keys, keys], axis=0).astype(bf16)
        states_in[h].wait()
        for p in range(seqs // 2):
            stacked = []
            for b in (2 * p, 2 * p + 1):
                mask = jnp.where(seq_of_lane == b, 1.0, 0.0).astype(bf16)
                update = jnp.dot(weighted * mask, key_pair, preferred_element_type=f32)
                state = shrink[h : h + 1, b : b + 1] * state_c_v[h, b] + update
                state_c_v[h, b] = state
                stacked.append(jnp.concatenate(split(state), axis=1))
            pair = slice(2 * p * props, 2 * (p + 1) * props)
            asked = query_f[pair].astype(bf16)
            found = dot_nt(
                jnp.concatenate([asked, asked], axis=1), jnp.concatenate(stacked, axis=0)
            )
            recall_v[pair, cols] = jnp.where(upper, found[:, :size], found[:, size:])
        copy = pltpu.make_async_copy(state_c_v.at[h], carried_c.at[:, h], out_sems.at[h])
        copy.start()
        out_copies.append(copy)

    new_keys = project(1)
    new_values = project(2)
    outgate = project(3)
    for h in range(heads):
        cols = slice(h * size, (h + 1) * size)
        query, key, value = queries[:, cols], new_keys[:, cols], new_values[:, cols]
        step_keys[:, h] = key.astype(f32).reshape(seqs, props, size).astype(bf16)
        step_values[:, h] = value.astype(f32).reshape(seqs, props, size).astype(bf16)
        c_col = cumul[:, heads_total + h : heads_total + h + 1]
        c_row = cumul_t[heads_total + h : heads_total + h + 1, :]
        i_row = gates_t[h : h + 1, :]
        logs_ts = jnp.where(causal, c_col - c_row + i_row, -jnp.inf)
        carried = c_col + stable_col[:, h : h + 1]
        steady = jnp.maximum(carried, jnp.max(logs_ts, axis=1, keepdims=True))
        scores = dot_nt(query, key) * scale * jnp.exp(logs_ts - steady)
        weight_state = jnp.exp(carried - steady)
        numer = weight_state * recall_v[:, cols] + jnp.dot(
            jnp.concatenate(split(scores), axis=1),
            jnp.concatenate([value, value], axis=0),
            preferred_element_type=f32,
        )
        denom = weight_state * recall_norm[h] + jnp.sum(scores, axis=1, keepdims=True)
        hidden = numer / jnp.maximum(jnp.abs(denom), jnp.exp(-steady))
        hidden = hidden * lax.rsqrt(jnp.mean(hidden * hidden, axis=1, keepdims=True) + EPSILON)
        hidden = hidden * head_gain_v[:, cols].astype(f32)
        gated_v[:, cols] = (hidden * jax.nn.sigmoid(outgate[:, cols].astype(f32))).astype(bf16)
    for chip in range(gated_out.shape[0]):
        copy = pltpu.make_async_copy(gated_v, gated_out.at[chip], out_sems.at[len(out_copies)])
        copy.start()
        out_copies.append(copy)
    arrive(out_copies)


def cell(
    tokens, norm_gain, query_weight, key_weight, value_weight, outgate_weight, gate_weight,
    gate_bias, head_gain, state_c, state_n, state_m, prev_keys, prev_values, prev_gates, accepted,
):
    f32, bf16 = jnp.float32, jnp.bfloat16
    seqs, props, width = tokens.shape
    heads, size = state_n.shape[1:]
    rows, columns = seqs * props, heads * size
    chips = lax.axis_size("kv") // 2
    inputs = (
        accepted,
        tokens,
        norm_gain.reshape(1, width),
        query_weight,
        key_weight,
        value_weight,
        outgate_weight,
        gate_weight.T,
        gate_bias,
        head_gain.reshape(1, columns),
        state_c,
        state_n,
        state_m.T,
        prev_keys,
        prev_values,
        prev_gates.transpose(1, 2, 3, 0),
    )
    outs = (
        jax.ShapeDtypeStruct((chips, rows, columns), bf16),
        jax.ShapeDtypeStruct(state_c.shape, f32),
        jax.ShapeDtypeStruct(state_n.shape, f32),
        jax.ShapeDtypeStruct((heads, seqs), f32),
        jax.ShapeDtypeStruct(prev_keys.shape, bf16),
        jax.ShapeDtypeStruct(prev_values.shape, bf16),
        jax.ShapeDtypeStruct((heads, 2, props, seqs), f32),
    )
    here = pl.BlockSpec(memory_space=pltpu.VMEM)
    anywhere = pl.BlockSpec(memory_space=pltpu.HBM)
    outputs = pl.pallas_call(
        cell_kernel,
        out_shape=outs,
        in_specs=[pl.BlockSpec(memory_space=pltpu.SMEM)] + [anywhere] * 15,
        out_specs=[anywhere, anywhere] + [here] * 5,
        scratch_shapes=[
            pltpu.VMEM(tokens.shape, bf16),
            pltpu.VMEM((1, width), bf16),
            pltpu.VMEM((4, width, columns), bf16),
            pltpu.VMEM(gate_weight.shape[::-1], bf16),
            pltpu.VMEM(gate_bias.shape, f32),
            pltpu.VMEM((1, columns), bf16),
            pltpu.VMEM((heads, seqs, size, size), f32),
            pltpu.VMEM(state_n.shape, f32),
            pltpu.VMEM((heads, seqs), f32),
            pltpu.VMEM(prev_keys.shape, bf16),
            pltpu.VMEM(prev_values.shape, bf16),
            pltpu.VMEM((heads, 2, props, seqs), f32),
            pltpu.VMEM((rows, width), f32),
            pltpu.VMEM((rows, width), bf16),
            pltpu.VMEM((rows, columns), f32),
            pltpu.VMEM((rows, columns), bf16),
            pltpu.SemaphoreType.DMA((10 + 16 + heads,)),
            pltpu.SemaphoreType.DMA((heads + chips,)),
        ],
        compiler_params=pltpu.CompilerParams(vmem_limit_bytes=62 * 1024 * 1024),
        cost_estimate=pl.CostEstimate(
            flops=2 * rows * width * 4 * columns, bytes_accessed=27 << 20, transcendentals=0
        ),
    )(*inputs)
    gated, new_c, new_n, new_m, keys, values, gates = outputs
    return gated, new_c, new_n, new_m.T, keys, values, gates.transpose(3, 0, 1, 2)


def per_device(*arrays):
    inputs, out_weight = arrays[:9] + arrays[10:], arrays[9]
    parts = passed_on(out_weight)
    sent, *rest = cell(*inputs)
    mixed = project_out(sent, parts)
    return (mixed.reshape(-1, inputs[0].shape[1], mixed.shape[1]), *rest)


def solution(mesh):
    in_specs = (
        P("kv", None, None),
        P(),
        P(None, "tp"),
        P(None, "tp"),
        P(None, "tp"),
        P(None, "tp"),
        P(),
        P(),
        P("tp"),
        P("tp", "kv"),
        P("kv", "tp", None, None),
        P("kv", "tp", None),
        P("kv", "tp"),
        P("kv", "tp", None, None),
        P("kv", "tp", None, None),
        P("kv", "tp", None, None),
        P("kv"),
    )
    out_specs = (
        P(None, None, "kv"),
        P("kv", "tp", None, None),
        P("kv", "tp", None),
        P("kv", "tp"),
        P("kv", "tp", None, None),
        P("kv", "tp", None, None),
        P("kv", "tp", None, None),
    )
    return jax.shard_map(
        per_device, mesh=mesh, in_specs=in_specs, out_specs=out_specs, check_vma=False
    )
```

time: 115 us -> 66.3 us (0.58)
  the two profiles are of different devices: /device:TPU:0 before, /device:TPU:1 now
where the time goes in v2:
time: 66.3 us; the launch traced here: 65.9 us
  starting transfers between devices  22.7 us (34%)
  Pallas kernels  15.7 us (24%)
  blocking collectives  11.9 us (18%)
  waiting for transfers between devices  11.5 us (17%)
  local copies, waits for them, and re-layouts  3.44 us (5%)
  between operations  0.68 us (1%)
    pallas_call x1, Pallas kernels, cell(): pl.pallas_call(cell_kernel, out_shape=outs, in_specs=[pl.BlockSpec(memory...  15.3 us
    all_to_all x1, starting transfers between devices, project_out(): lax.all_to_all(sent.reshape(chips * tp, rows, depth), ('kv', 'tp'), 0, 0,...  12 us
    all_to_all x1, blocking collectives, project_out(): lax.all_to_all(mixed.reshape(2 * tp, chips * rows, columns), ('kv', 'tp')...  11.9 us
    ppermute x3, waiting for transfers between devices, passed_on(): lax.ppermute(weight, 'tp', ring(tp, step))  10.1 us
    ppermute x4, starting transfers between devices, swap_cores(): lax.ppermute(x, 'kv', [(i, i ^ 1) for i in range(lax.axis_size('kv'))])  6.06 us
    ppermute x3, starting transfers between devices, passed_on(): lax.ppermute(weight, 'tp', ring(tp, step))  4.66 us
    ppermute x4, waiting for transfers between devices, swap_cores(): lax.ppermute(x, 'kv', [(i, i ^ 1) for i in range(lax.axis_size('kv'))])  1.33 us
  transfers between devices with their start and end apart: 8, of which 4 were waited for; matrix products, arithmetic and copies ran while one was open for 0% of the time, Pallas kernels for 0%

profile of v2, /device:TPU:1, one launch (start us, length us, event | category | flops | bytes accessed | tf_op | source)
XLA Modules:
  0.0 65.9 jit_solution(8626996052311333112)
XLA Ops:
  0.6 1.3 %reshape.32.norm_gain = bf16[1,4096]{1,0:T(2,128)(2,1)} reshape(bf16[4096]{0:T(1024)(128)(2,1)} %param.18) | data formatting | bytes 16384 | tf_op jit(solution)/shard_map/reshape | solution.py:362
  1.9 1.3 %reshape.33.head_gain = bf16[1,512]{1,0:T(2,128)(2,1)} reshape(bf16[512]{0:T(512)(128)(2,1)} %param.25) | data formatting | bytes 2048 | tf_op jit(solution)/shard_map/reshape | solution.py:369
  3.2 0.0 copy-start
  3.2 15.3 %shard_map.216 = (bf16[16,64,512]{2,1,0:T(8,128)(2,1)}, f32[16,4,128,128]{3,2,1,0:T(8,128)}, f32[16,4,128]{2,1,0:T(4,128)}, f32[4,16]{1,0:T(4,128)}, bf16[16,4,4...) custom-call(s32[16]{0:T(128)} %accepted.1, bf16[16,4,4096]{2,1,0:T(4,128)(2,1)} %tokens.1, ...), custom_call_target="tpu_custom_call" | custom-call | flops 1073741824 | bytes 28311552 | tf_op jit(solution)/shard_map/pallas_call | solution.py:388
  18.5 12.0 %all-to-all-start = ((bf16[64,16,512]{2,1,0:T(8,128)(2,1)}), bf16[64,16,512]{2,1,0:T(8,128)(2,1)S(1)}, u32[]{:S(2)}, u32[]{:S(2)}) async-start(bf16[64,16,512]{2,1,0:T(8,128)(2,1)} %bitcast.15), calls=%async_computation | async-start | bytes 2097152 | tf_op jit(solution)/shard_map/all_to_all | solution.py:64
  30.5 0.0 copy-done
  30.5 1.1 %collective-permute-start = (bf16[512,128]{1,0:T(8,128)(2,1)S(1)}, bf16[512,128]{1,0:T(8,128)(2,1)S(1)}, u32[]{:S(2)}, u32[]{:S(2)}) collective-permute-start(bf16[512,128]{1,0:T(8,128)(2,1)S(1)} %copy-done), channel_id=1, source_target_pairs={{0,1},{1,2},{2,3},{3,0},{4,5},{5,6},{6,7},{7,4},{8,9},{9,10},{10,1... | collective-permute-start | bytes 393224 | tf_op jit(solution)/shard_map/ppermute | solution.py:23
  31.6 2.4 %collective-permute-start.1 = (bf16[512,128]{1,0:T(8,128)(2,1)S(1)}, bf16[512,128]{1,0:T(8,128)(2,1)S(1)}, u32[]{:S(2)}, u32[]{:S(2)}) collective-permute-start(bf16[512,128]{1,0:T(8,128)(2,1)S(1)} %copy-done), channel_id=1, source_target_pairs={{0,2},{1,3},{2,0},{3,1},{4,6},{5,7},{6,4},{7,5},{8,10},{9,11},{10,... | collective-permute-start | bytes 393224 | tf_op jit(solution)/shard_map/ppermute | solution.py:23
  34.0 1.2 %collective-permute-start.2 = (bf16[512,128]{1,0:T(8,128)(2,1)S(1)}, bf16[512,128]{1,0:T(8,128)(2,1)S(1)}, u32[]{:S(2)}, u32[]{:S(2)}) collective-permute-start(bf16[512,128]{1,0:T(8,128)(2,1)S(1)} %copy-done), channel_id=1, source_target_pairs={{0,3},{1,0},{2,1},{3,2},{4,7},{5,4},{6,5},{7,6},{8,11},{9,8},{10,9... | collective-permute-start | bytes 393224 | tf_op jit(solution)/shard_map/ppermute | solution.py:23
  35.2 2.1 %collective-permute-start.3 = (bf16[512,128]{1,0:T(8,128)(2,1)S(1)}, bf16[512,128]{1,0:T(8,128)(2,1)S(1)}, u32[]{:S(2)}, u32[]{:S(2)}) collective-permute-start(bf16[512,128]{1,0:T(8,128)(2,1)S(1)} %copy-done), channel_id=1, source_target_pairs={{0,4},{4,0},{8,12},{12,8},{16,20},{20,16},{24,28},{28,24},{32,36},... | collective-permute-start | bytes 393224 | tf_op jit(solution)/shard_map/ppermute | solution.py:18
  37.2 9.9 %collective-permute-done.refs_1_ = bf16[512,128]{1,0:T(8,128)(2,1)S(1)} collective-permute-done((bf16[512,128]{1,0:T(8,128)(2,1)S(1)}, bf16[512,128]{1,0:T(8,128)(2,1)S(1)}, u32[]{:S(2)}, u32[]{:S(2)}) %collective-permute-start) | collective-permute-done | bytes 131104 | tf_op jit(solution)/shard_map/ppermute | solution.py:23
  47.2 2.2 %collective-permute-start.4 = (bf16[512,128]{1,0:T(8,128)(2,1)S(1)}, bf16[512,128]{1,0:T(8,128)(2,1)S(1)}, u32[]{:S(2)}, u32[]{:S(2)}) collective-permute-start(bf16[512,128]{1,0:T(8,128)(2,1)S(1)} %collective-permute-done.refs_1_), channel_id=1, source_target_pairs={{0,4},{4,0},{8,12},{12,8},{16,20},{20,16},{24,28},{28,24},{32,36},... | collective-permute-start | bytes 393224 | tf_op jit(solution)/shard_map/ppermute | solution.py:18
  49.4 0.2 collective-permute-done.1.refs_2_
  49.5 1.8 %collective-permute-start.5 = (bf16[512,128]{1,0:T(8,128)(2,1)S(1)}, bf16[512,128]{1,0:T(8,128)(2,1)S(1)}, u32[]{:S(2)}, u32[]{:S(2)}) collective-permute-start(bf16[512,128]{1,0:T(8,128)(2,1)S(1)} %collective-permute-done.1.refs_2_), channel_id=1, source_target_pairs={{0,4},{4,0},{8,12},{12,8},{16,20},{20,16},{24,28},{28,24},{32,36},... | collective-permute-start | bytes 393224 | tf_op jit(solution)/shard_map/ppermute | solution.py:18
  51.3 0.0 collective-permute-done.2.refs_3_
  51.3 0.0 collective-permute-start.6
  51.4 0.0 collective-permute-done.3.refs_4_
  51.4 0.0 collective-permute-done.4.refs_5_
  51.4 1.0 %collective-permute-done.5.refs_6_ = bf16[512,128]{1,0:T(8,128)(2,1)S(1)} collective-permute-done((bf16[512,128]{1,0:T(8,128)(2,1)S(1)}, bf16[512,128]{1,0:T(8,128)(2,1)S(1)}, u32[]{:S(2)}, u32[]{:S(2)}) %collective-permute-start.5) | collective-permute-done | bytes 131104 | tf_op jit(solution)/shard_map/ppermute | solution.py:18
  52.3 0.4 collective-permute-done.6.refs_7_
  52.7 0.0 all-to-all-done
  52.7 0.4 shard_map.217
  53.1 11.9 %all_to_all.10 = bf16[8,256,128]{2,1,0:T(8,128)(2,1)S(1)} all-to-all(bf16[8,256,128]{2,1,0:T(8,128)(2,1)S(1)} %bitcast.13), channel_id=1, replica_groups={{0,1,2,3,4,5,6,7},{8,9,10,11,12,13,14,15},{16,17,18,19,20,21,22,23},{24..., dimensions={0} | all-to-all | bytes 1048576 | tf_op jit(solution)/shard_map/all_to_all | solution.py:79
  65.1 0.9 %copy.24 = bf16[2,4,16,16,128]{4,3,1,0,2:T(8,128)(2,1)} copy(bf16[2,4,16,16,128]{4,3,2,1,0:T(8,128)(2,1)S(1)} %bitcast.14) | data formatting | bytes 1048576 | tf_op jit(solution)/shard_map/reshape | solution.py:82
Async XLA Ops:
  3.2 27.3 %copy-start = (bf16[512,128]{1,0:T(8,128)(2,1)S(1)}, bf16[512,128]{1,0:T(8,128)(2,1)}, u32[]{:S(2)}) copy-start(bf16[512,128]{1,0:T(8,128)(2,1)} %refs_0_.1) | copy-start | bytes 393220
  18.5 34.2 %all-to-all-start = ((bf16[64,16,512]{2,1,0:T(8,128)(2,1)}), bf16[64,16,512]{2,1,0:T(8,128)(2,1)S(1)}, u32[]{:S(2)}, u32[]{:S(2)}) async-start(bf16[64,16,512]{2,1,0:T(8,128)(2,1)} %bitcast.15), calls=%async_computation | async-start | bytes 2097152 | tf_op jit(solution)/shard_map/all_to_all | solution.py:64
  30.5 16.7 %collective-permute-start = (bf16[512,128]{1,0:T(8,128)(2,1)S(1)}, bf16[512,128]{1,0:T(8,128)(2,1)S(1)}, u32[]{:S(2)}, u32[]{:S(2)}) collective-permute-start(bf16[512,128]{1,0:T(8,128)(2,1)S(1)} %copy-done), channel_id=1, source_target_pairs={{0,1},{1,2},{2,3},{3,0},{4,5},{5,6},{6,7},{7,4},{8,9},{9,10},{10,1... | collective-permute-start | bytes 393224 | tf_op jit(solution)/shard_map/ppermute | solution.py:23
  31.6 17.9 %collective-permute-start.1 = (bf16[512,128]{1,0:T(8,128)(2,1)S(1)}, bf16[512,128]{1,0:T(8,128)(2,1)S(1)}, u32[]{:S(2)}, u32[]{:S(2)}) collective-permute-start(bf16[512,128]{1,0:T(8,128)(2,1)S(1)} %copy-done), channel_id=1, source_target_pairs={{0,2},{1,3},{2,0},{3,1},{4,6},{5,7},{6,4},{7,5},{8,10},{9,11},{10,... | collective-permute-start | bytes 393224 | tf_op jit(solution)/shard_map/ppermute | solution.py:23
  34.0 17.4 %collective-permute-start.2 = (bf16[512,128]{1,0:T(8,128)(2,1)S(1)}, bf16[512,128]{1,0:T(8,128)(2,1)S(1)}, u32[]{:S(2)}, u32[]{:S(2)}) collective-permute-start(bf16[512,128]{1,0:T(8,128)(2,1)S(1)} %copy-done), channel_id=1, source_target_pairs={{0,3},{1,0},{2,1},{3,2},{4,7},{5,4},{6,5},{7,6},{8,11},{9,8},{10,9... | collective-permute-start | bytes 393224 | tf_op jit(solution)/shard_map/ppermute | solution.py:23
  35.2 16.2 %collective-permute-start.3 = (bf16[512,128]{1,0:T(8,128)(2,1)S(1)}, bf16[512,128]{1,0:T(8,128)(2,1)S(1)}, u32[]{:S(2)}, u32[]{:S(2)}) collective-permute-start(bf16[512,128]{1,0:T(8,128)(2,1)S(1)} %copy-done), channel_id=1, source_target_pairs={{0,4},{4,0},{8,12},{12,8},{16,20},{20,16},{24,28},{28,24},{32,36},... | collective-permute-start | bytes 393224 | tf_op jit(solution)/shard_map/ppermute | solution.py:18
  47.2 4.2 %collective-permute-start.4 = (bf16[512,128]{1,0:T(8,128)(2,1)S(1)}, bf16[512,128]{1,0:T(8,128)(2,1)S(1)}, u32[]{:S(2)}, u32[]{:S(2)}) collective-permute-start(bf16[512,128]{1,0:T(8,128)(2,1)S(1)} %collective-permute-done.refs_1_), channel_id=1, source_target_pairs={{0,4},{4,0},{8,12},{12,8},{16,20},{20,16},{24,28},{28,24},{32,36},... | collective-permute-start | bytes 393224 | tf_op jit(solution)/shard_map/ppermute | solution.py:18
  49.5 2.8 %collective-permute-start.5 = (bf16[512,128]{1,0:T(8,128)(2,1)S(1)}, bf16[512,128]{1,0:T(8,128)(2,1)S(1)}, u32[]{:S(2)}, u32[]{:S(2)}) collective-permute-start(bf16[512,128]{1,0:T(8,128)(2,1)S(1)} %collective-permute-done.1.refs_2_), channel_id=1, source_target_pairs={{0,4},{4,0},{8,12},{12,8},{16,20},{20,16},{24,28},{28,24},{32,36},... | collective-permute-start | bytes 393224 | tf_op jit(solution)/shard_map/ppermute | solution.py:18
  51.3 1.3 %collective-permute-start.6 = (bf16[512,128]{1,0:T(8,128)(2,1)S(1)}, bf16[512,128]{1,0:T(8,128)(2,1)S(1)}, u32[]{:S(2)}, u32[]{:S(2)}) collective-permute-start(bf16[512,128]{1,0:T(8,128)(2,1)S(1)} %collective-permute-done.2.refs_3_), channel_id=1, source_target_pairs={{0,4},{4,0},{8,12},{12,8},{16,20},{20,16},{24,28},{28,24},{32,36},... | collective-permute-start | bytes 393224 | tf_op jit(solution)/shard_map/ppermute | solution.py:18

commit v3 on v2

--- a/solution.py
+++ b/solution.py
@@ -109,6 +109,61 @@
     return lax.broadcasted_iota(jnp.int32, shape, dim)
 
 
+def bringer(sems):
+    copies = []
+
+    def bring(src, dst):
+        copy = pltpu.make_async_copy(src, dst, sems.at[len(copies)])
+        copies.append(copy)
+        copy.start()
+        return copy
+
+    return bring
+
+
+def arrive(some):
+    for copy in some:
+        copy.wait()
+
+
+def spreads(seqs, rows):
+    across = jnp.where(iota((seqs, rows), 0) == (iota((seqs, rows), 1) >> 2), 1.0, 0.0)
+    down = jnp.where((iota((rows, seqs), 0) >> 2) == iota((rows, seqs), 1), 1.0, 0.0)
+    return across, down
+
+
+def replay(accepted, state_m, prev_gates, across):
+    heads, _, props, seqs = prev_gates.shape
+    seq_lane = iota((1, seqs), 1)
+    counts = jnp.zeros((1, seqs), jnp.int32)
+    for b in range(seqs):
+        counts = jnp.where(seq_lane == b, accepted[b], counts)
+    total = jnp.zeros((heads, seqs), jnp.float32)
+    sums, inputs = [], []
+    for s in range(props):
+        both = [
+            jnp.concatenate([prev_gates[h, g, s : s + 1, :] for h in range(heads)], axis=0)
+            for g in (0, 1)
+        ]
+        total = total + jnp.where(counts > s, log_sigmoid(both[1]), 0.0)
+        sums.append(total)
+        inputs.append(both[0])
+    logs = [
+        jnp.where(counts > s, total - sums[s] + inputs[s], -jnp.inf) for s in range(props)
+    ]
+    decayed = total + state_m[...]
+    stable = decayed
+    for s in range(props):
+        stable = jnp.maximum(stable, logs[s])
+    shrink = jnp.exp(decayed - stable)
+    prop_lane = iota((1, across.shape[1]), 1) & (props - 1)
+    weights = jnp.zeros((heads, across.shape[1]), jnp.float32)
+    for s in range(props):
+        spaced = exact_dot(jnp.exp(logs[s] - stable), across, (1, 0))
+        weights = weights + jnp.where(prop_lane == s, spaced, 0.0)
+    return stable, shrink, weights
+
+
 def cell_kernel(
     accepted,
     tokens,
@@ -127,12 +182,10 @@
     prev_values,
     prev_gates,
     gated_out,
-    carried_c,
-    carried_n,
-    carried_m,
-    step_keys,
-    step_values,
-    step_gates,
+    keys_out,
+    values_out,
+    gates_out,
+    accepted_s,
     tokens_v,
     gain_v,
     weights_v,
@@ -148,6 +201,7 @@
     normed_f,
     normed_v,
     recall_v,
+    hidden_v,
     gated_v,
     sems,
     out_sems,
@@ -160,14 +214,7 @@
     scale = size ** (-0.5)
     pieces = 4
     depth = width // pieces
-
-    copies = []
-
-    def bring(src, dst):
-        copy = pltpu.make_async_copy(src, dst, sems.at[len(copies)])
-        copies.append(copy)
-        copy.start()
-        return copy
+    bring = bringer(sems)
 
     def bring_weight(which, src):
         return [
@@ -178,6 +225,7 @@
     early = [bring(tokens, tokens_v), bring(norm_gain, gain_v)]
     gates_in = [bring(gate_weight, gate_weight_v), bring(gate_bias, gate_bias_v)]
     replay_in = [
+        bring(accepted, accepted_s),
         bring(state_m, state_m_v),
         bring(prev_gates, prev_gates_v),
         bring(state_n, state_n_v),
@@ -193,20 +241,13 @@
         bring_weight(3, outgate_weight),
     ]
 
-    def arrive(some):
-        for copy in some:
-            copy.wait()
-
-    row_lane = iota((1, rows), 1)
-    prop_lane = row_lane & (props - 1)
-    spread = jnp.where(iota((seqs, rows), 0) == (iota((seqs, rows), 1) >> 2), 1.0, 0.0)
-    spread_t = jnp.where((iota((rows, seqs), 0) >> 2) == iota((rows, seqs), 1), 1.0, 0.0)
+    across, down = spreads(seqs, rows)
     square = (rows, rows)
     same = (iota(square, 0) >> 2) == (iota(square, 1) >> 2)
     causal = same & (iota(square, 0) >= iota(square, 1))
 
     arrive(early)
-    gain = gain_v[...].astype(f32)
+    gain = gain_v[...].astype(f32).reshape(1, width)
     for b in range(seqs):
         x = tokens_v[b].astype(f32)
         mean = jnp.mean(x * x, axis=-1, keepdims=True)
@@ -219,49 +260,16 @@
     gates = jnp.concatenate([gates, jnp.zeros((rows, 128 - 2 * heads_total), f32)], axis=1)
     first_head = lax.axis_index("tp") * heads
     gates = pltpu.roll(gates, 128 - first_head, 1)
-    forget = log_sigmoid(gates)
-    cumul = exact_dot(jnp.where(causal, 1.0, 0.0), forget, (1, 0))
+    cumul = exact_dot(jnp.where(causal, 1.0, 0.0), log_sigmoid(gates), (1, 0))
     gates_t = gates.T
     cumul_t = cumul.T
-    for t in range(props):
-        pick = jnp.where(iota((rows, seqs), 0) == iota((rows, seqs), 1) * props + t, 1.0, 0.0)
-        picked = exact_dot(gates_t[: 2 * heads_total], pick, (1, 0))
-        for h in range(heads):
-            step_gates[h, 0, t : t + 1, :] = picked[h : h + 1, :]
-            step_gates[h, 1, t : t + 1, :] = picked[heads_total + h : heads_total + h + 1, :]
+    gates_out[...] = gates_t[: 2 * heads_total]
 
     arrive(replay_in)
-    seq_lane = iota((1, seqs), 1)
-    counts = jnp.zeros((1, seqs), jnp.int32)
-    for b in range(seqs):
-        counts = jnp.where(seq_lane == b, accepted[b], counts)
-    total = jnp.zeros((heads, seqs), f32)
-    sums, inputs = [], []
-    for s in range(props):
-        both = [
-            jnp.concatenate([prev_gates_v[h, g, s : s + 1, :] for h in range(heads)], axis=0)
-            for g in (0, 1)
-        ]
-        total = total + jnp.where(counts > s, log_sigmoid(both[1]), 0.0)
-        sums.append(total)
-        inputs.append(both[0])
-    logs = [
-        jnp.where(counts > s, total - sums[s] + inputs[s], -jnp.inf) for s in range(props)
-    ]
-    decayed = total + state_m_v[...]
-    stable = decayed
-    for s in range(props):
-        stable = jnp.maximum(stable, logs[s])
-    carried_m[...] = stable
-    shrink = jnp.exp(decayed - stable)
-    weights = jnp.zeros((heads, rows), f32)
-    for s in range(props):
-        spaced = exact_dot(jnp.exp(logs[s] - stable), spread, (1, 0))
-        weights = weights + jnp.where(prop_lane == s, spaced, 0.0)
+    stable, shrink, weights = replay(accepted_s, state_m_v, prev_gates_v, across)
     weights = weights * scale
-    stable_col = exact_dot(spread_t, stable, (1, 1))
-    diagonal = jnp.where(iota((seqs, seqs), 0) == iota((seqs, seqs), 1), 1.0, 0.0)
-    shrink_col = exact_dot(diagonal, shrink, (1, 1))
+    stable_col = exact_dot(down, stable, (1, 1))
+    shrink_col = exact_dot(down, shrink, (1, 1))
 
     def project(which):
         acc = None
@@ -276,75 +284,133 @@
         return acc.astype(bf16)
 
     queries = project(0)
-    out_copies = []
-    seq_of_lane = (iota((1, 2 * rows), 1) & (rows - 1)) >> 2
     upper = iota((2 * props, size), 0) < props
-    recall_norm = []
     for h in range(heads):
         cols = slice(h * size, (h + 1) * size)
-        query = queries[:, cols]
-        query_f = query.astype(f32)
-        keys = prev_keys_v[:, h].astype(f32).reshape(rows, size)
-        values = prev_values_v[:, h].astype(f32).reshape(rows, size)
-        weight = weights[h : h + 1, :]
-        norm = shrink_col[:, h : h + 1] * state_n_v[:, h, :] + exact_dot(
-            spread * weight, keys, (1, 0)
-        )
-        carried_n[:, h, :] = norm
-        along = exact_dot(query_f, norm, (1, 1))
-        recall_norm.append(jnp.sum(along * spread_t, axis=1, keepdims=True))
-        weighted = jnp.concatenate(split(values.T * weight), axis=1)
-        key_pair = jnp.concatenate([keys, keys], axis=0).astype(bf16)
+        query_f = queries[:, cols].astype(f32)
         states_in[h].wait()
         for p in range(seqs // 2):
-            stacked = []
-            for b in (2 * p, 2 * p + 1):
-                mask = jnp.where(seq_of_lane == b, 1.0, 0.0).astype(bf16)
-                update = jnp.dot(weighted * mask, key_pair, preferred_element_type=f32)
-                state = shrink[h : h + 1, b : b + 1] * state_c_v[h, b] + update
-                state_c_v[h, b] = state
-                stacked.append(jnp.concatenate(split(state), axis=1))
+            stacked = [
+                jnp.concatenate(split(state_c_v[h, b]), axis=1) for b in (2 * p, 2 * p + 1)
+            ]
             pair = slice(2 * p * props, 2 * (p + 1) * props)
             asked = query_f[pair].astype(bf16)
             found = dot_nt(
                 jnp.concatenate([asked, asked], axis=1), jnp.concatenate(stacked, axis=0)
             )
             recall_v[pair, cols] = jnp.where(upper, found[:, :size], found[:, size:])
-        copy = pltpu.make_async_copy(state_c_v.at[h], carried_c.at[:, h], out_sems.at[h])
-        copy.start()
-        out_copies.append(copy)
 
     new_keys = project(1)
+    keys_out[...] = new_keys
     new_values = project(2)
-    outgate = project(3)
+    values_out[...] = new_values
     for h in range(heads):
         cols = slice(h * size, (h + 1) * size)
         query, key, value = queries[:, cols], new_keys[:, cols], new_values[:, cols]
-        step_keys[:, h] = key.astype(f32).reshape(seqs, props, size).astype(bf16)
-        step_values[:, h] = value.astype(f32).reshape(seqs, props, size).astype(bf16)
+        old_key = prev_keys_v[:, h].astype(f32).reshape(rows, size).astype(bf16)
+        old_value = prev_values_v[:, h].astype(f32).reshape(rows, size).astype(bf16)
         c_col = cumul[:, heads_total + h : heads_total + h + 1]
         c_row = cumul_t[heads_total + h : heads_total + h + 1, :]
         i_row = gates_t[h : h + 1, :]
         logs_ts = jnp.where(causal, c_col - c_row + i_row, -jnp.inf)
         carried = c_col + stable_col[:, h : h + 1]
         steady = jnp.maximum(carried, jnp.max(logs_ts, axis=1, keepdims=True))
+        weight_state = jnp.exp(carried - steady)
         scores = dot_nt(query, key) * scale * jnp.exp(logs_ts - steady)
-        weight_state = jnp.exp(carried - steady)
-        numer = weight_state * recall_v[:, cols] + jnp.dot(
-            jnp.concatenate(split(scores), axis=1),
-            jnp.concatenate([value, value], axis=0),
+        replayed = jnp.where(same, dot_nt(query, old_key) * weights[h : h + 1, :], 0.0)
+        both = jnp.concatenate([weight_state * replayed, scores], axis=1)
+        kept = weight_state * shrink_col[:, h : h + 1]
+        numer = kept * recall_v[:, cols] + jnp.dot(
+            jnp.concatenate(split(both), axis=1),
+            jnp.concatenate([old_value, value] * 2, axis=0),
             preferred_element_type=f32,
         )
-        denom = weight_state * recall_norm[h] + jnp.sum(scores, axis=1, keepdims=True)
+        along = exact_dot(query.astype(f32), state_n_v[:, h, :], (1, 1))
+        recall_norm = jnp.sum(along * down, axis=1, keepdims=True)
+        denom = kept * recall_norm + jnp.sum(both, axis=1, keepdims=True)
         hidden = numer / jnp.maximum(jnp.abs(denom), jnp.exp(-steady))
-        hidden = hidden * lax.rsqrt(jnp.mean(hidden * hidden, axis=1, keepdims=True) + EPSILON)
-        hidden = hidden * head_gain_v[:, cols].astype(f32)
-        gated_v[:, cols] = (hidden * jax.nn.sigmoid(outgate[:, cols].astype(f32))).astype(bf16)
-    for chip in range(gated_out.shape[0]):
-        copy = pltpu.make_async_copy(gated_v, gated_out.at[chip], out_sems.at[len(out_copies)])
+        hidden_v[:, cols] = hidden * lax.rsqrt(
+            jnp.mean(hidden * hidden, axis=1, keepdims=True) + EPSILON
+        )
+
+    outgate = project(3)
+    head_scale = head_gain_v[...].astype(f32).reshape(1, heads * size)
+    gated_v[...] = (
+        hidden_v[...] * head_scale * jax.nn.sigmoid(outgate.astype(f32))
+    ).astype(bf16)
+    sends = [
+        pltpu.make_async_copy(gated_v, gated_out.at[chip], out_sems.at[chip])
+        for chip in range(gated_out.shape[0])
+    ]
+    for copy in sends:
         copy.start()
-        out_copies.append(copy)
-    arrive(out_copies)
+    arrive(sends)
+
+
+def keep_kernel(
+    accepted,
+    state_c,
+    state_n,
+    state_m,
+    prev_keys,
+    prev_values,
+    prev_gates,
+    new_keys,
+    new_values,
+    gates_t,
+    carried_c,
+    carried_n,
+    carried_m,
+    step_keys,
+    step_values,
+    step_gates,
+    state_c_v,
+    sems,
+    out_sems,
+):
+    f32, bf16 = jnp.float32, jnp.bfloat16
+    heads, seqs, size, _ = state_c_v.shape
+    props = prev_gates.shape[2]
+    rows = seqs * props
+    scale = size ** (-0.5)
+    bring = bringer(sems)
+    states_in = [bring(state_c.at[:, h], state_c_v.at[h]) for h in range(heads)]
+    across, _ = spreads(seqs, rows)
+    for t in range(props):
+        pick = jnp.where(iota((rows, seqs), 0) == iota((rows, seqs), 1) * props + t, 1.0, 0.0)
+        picked = exact_dot(gates_t[...], pick, (1, 0))
+        total = picked.shape[0] // 2
+        for h in range(heads):
+            step_gates[h, 0, t : t + 1, :] = picked[h : h + 1, :]
+            step_gates[h, 1, t : t + 1, :] = picked[total + h : total + h + 1, :]
+    stable, shrink, weights = replay(accepted, state_m, prev_gates, across)
+    weights = weights * scale
+    carried_m[...] = stable
+    diagonal = jnp.where(iota((seqs, seqs), 0) == iota((seqs, seqs), 1), 1.0, 0.0)
+    shrink_col = exact_dot(diagonal, shrink, (1, 1))
+    seq_of_lane = (iota((1, 2 * rows), 1) & (rows - 1)) >> 2
+    outs = []
+    for h in range(heads):
+        cols = slice(h * size, (h + 1) * size)
+        step_keys[:, h] = new_keys[:, cols].astype(f32).reshape(seqs, props, size).astype(bf16)
+        step_values[:, h] = new_values[:, cols].astype(f32).reshape(seqs, props, size).astype(bf16)
+        keys = prev_keys[:, h].astype(f32).reshape(rows, size)
+        values = prev_values[:, h].astype(f32).reshape(rows, size)
+        weight = weights[h : h + 1, :]
+        carried_n[:, h, :] = shrink_col[:, h : h + 1] * state_n[:, h, :] + exact_dot(
+            across * weight, keys, (1, 0)
+        )
+        weighted = jnp.concatenate(split(values.T * weight), axis=1)
+        key_pair = jnp.concatenate([keys, keys], axis=0).astype(bf16)
+        states_in[h].wait()
+        for b in range(seqs):
+            mask = jnp.where(seq_of_lane == b, 1.0, 0.0).astype(bf16)
+            update = jnp.dot(weighted * mask, key_pair, preferred_element_type=f32)
+            state_c_v[h, b] = shrink[h : h + 1, b : b + 1] * state_c_v[h, b] + update
+        copy = pltpu.make_async_copy(state_c_v.at[h], carried_c.at[:, h], out_sems.at[h])
+        copy.start()
+        outs.append(copy)
+    arrive(outs)
 
 
 def cell(
@@ -359,14 +425,14 @@
     inputs = (
         accepted,
         tokens,
-        norm_gain.reshape(1, width),
+        norm_gain,
         query_weight,
         key_weight,
         value_weight,
         outgate_weight,
         gate_weight.T,
         gate_bias,
-        head_gain.reshape(1, columns),
+        head_gain,
         state_c,
         state_n,
         state_m.T,
@@ -374,29 +440,26 @@
         prev_values,
         prev_gates.transpose(1, 2, 3, 0),
     )
-    outs = (
-        jax.ShapeDtypeStruct((chips, rows, columns), bf16),
-        jax.ShapeDtypeStruct(state_c.shape, f32),
-        jax.ShapeDtypeStruct(state_n.shape, f32),
-        jax.ShapeDtypeStruct((heads, seqs), f32),
-        jax.ShapeDtypeStruct(prev_keys.shape, bf16),
-        jax.ShapeDtypeStruct(prev_values.shape, bf16),
-        jax.ShapeDtypeStruct((heads, 2, props, seqs), f32),
-    )
     here = pl.BlockSpec(memory_space=pltpu.VMEM)
-    anywhere = pl.BlockSpec(memory_space=pltpu.HBM)
-    outputs = pl.pallas_call(
+    anywhere = pl.BlockSpec(memory_space=pl.ANY)
+    sent, *fresh = pl.pallas_call(
         cell_kernel,
-        out_shape=outs,
-        in_specs=[pl.BlockSpec(memory_space=pltpu.SMEM)] + [anywhere] * 15,
-        out_specs=[anywhere, anywhere] + [here] * 5,
+        out_shape=(
+            jax.ShapeDtypeStruct((chips, rows, columns), bf16),
+            jax.ShapeDtypeStruct((rows, columns), bf16),
+            jax.ShapeDtypeStruct((rows, columns), bf16),
+            jax.ShapeDtypeStruct((gate_weight.shape[1], rows), f32),
+        ),
+        in_specs=[anywhere] * 16,
+        out_specs=[anywhere] + [here] * 3,
         scratch_shapes=[
+            pltpu.SMEM(accepted.shape, jnp.int32),
             pltpu.VMEM(tokens.shape, bf16),
-            pltpu.VMEM((1, width), bf16),
+            pltpu.VMEM((width,), bf16),
             pltpu.VMEM((4, width, columns), bf16),
             pltpu.VMEM(gate_weight.shape[::-1], bf16),
             pltpu.VMEM(gate_bias.shape, f32),
-            pltpu.VMEM((1, columns), bf16),
+            pltpu.VMEM((columns,), bf16),
             pltpu.VMEM((heads, seqs, size, size), f32),
             pltpu.VMEM(state_n.shape, f32),
             pltpu.VMEM((heads, seqs), f32),
@@ -406,17 +469,39 @@
             pltpu.VMEM((rows, width), f32),
             pltpu.VMEM((rows, width), bf16),
             pltpu.VMEM((rows, columns), f32),
+            pltpu.VMEM((rows, columns), f32),
             pltpu.VMEM((rows, columns), bf16),
-            pltpu.SemaphoreType.DMA((10 + 16 + heads,)),
-            pltpu.SemaphoreType.DMA((heads + chips,)),
+            pltpu.SemaphoreType.DMA((11 + 16 + heads,)),
+            pltpu.SemaphoreType.DMA((chips,)),
         ],
         compiler_params=pltpu.CompilerParams(vmem_limit_bytes=62 * 1024 * 1024),
         cost_estimate=pl.CostEstimate(
-            flops=2 * rows * width * 4 * columns, bytes_accessed=27 << 20, transcendentals=0
+            flops=2 * rows * width * 4 * columns, bytes_accessed=22 << 20, transcendentals=0
         ),
     )(*inputs)
-    gated, new_c, new_n, new_m, keys, values, gates = outputs
-    return gated, new_c, new_n, new_m.T, keys, values, gates.transpose(3, 0, 1, 2)
+    new_c, new_n, new_m, keys, values, gates = pl.pallas_call(
+        keep_kernel,
+        out_shape=(
+            jax.ShapeDtypeStruct(state_c.shape, f32),
+            jax.ShapeDtypeStruct(state_n.shape, f32),
+            jax.ShapeDtypeStruct((heads, seqs), f32),
+            jax.ShapeDtypeStruct(prev_keys.shape, bf16),
+            jax.ShapeDtypeStruct(prev_values.shape, bf16),
+            jax.ShapeDtypeStruct((heads, 2, props, seqs), f32),
+        ),
+        in_specs=[pl.BlockSpec(memory_space=pltpu.SMEM), anywhere] + [here] * 8,
+        out_specs=[anywhere] + [here] * 5,
+        scratch_shapes=[
+            pltpu.VMEM((heads, seqs, size, size), f32),
+            pltpu.SemaphoreType.DMA((heads,)),
+            pltpu.SemaphoreType.DMA((heads,)),
+        ],
+        compiler_params=pltpu.CompilerParams(vmem_limit_bytes=58 * 1024 * 1024),
+        cost_estimate=pl.CostEstimate(
+            flops=2 * heads * seqs * size * size * 64, bytes_accessed=9 << 20, transcendentals=0
+        ),
+    )(accepted, state_c, state_n, inputs[12], prev_keys, prev_values, inputs[15], *fresh)
+    return sent, new_c, new_n, new_m.T, keys, values, gates.transpose(3, 0, 1, 2)
 
 
 def per_device(*arrays):

time: 66.3 us -> 61 us (0.920)
  blocking collectives: 11.9 us -> 0 us
  starting transfers between devices: 22.7 us -> 27.1 us
  waiting for transfers between devices: 11.5 us -> 14.1 us
  local copies, waits for them, and re-layouts: 3.44 us -> 0.86 us
  Pallas kernels: 15.7 us -> 17.9 us
    all_to_all x1 -> x0, blocking collectives: 11.9 us -> none  [project_out(): lax.all_to_all(mixed.reshape(2 * tp, chips * rows, columns), ('kv', 'tp')...]
    all_to_all x0 -> x1, waiting for transfers between devices: none -> 3.97 us  [project_out(): lax.all_to_all(mixed.reshape(2 * tp, chips * rows, columns), ('kv', 'tp')...]
    all_to_all x0 -> x1, starting transfers between devices: none -> 3.78 us  [project_out(): lax.all_to_all(mixed.reshape(2 * tp, chips * rows, columns), ('kv', 'tp')...]
    reshape x2 -> x0, local copies, waits for them, and re-layouts: 2.58 us -> none  [the longest x1 1.31 us: cell(): norm_gain.reshape(1, width)]
    ppermute x4, starting transfers between devices: 6.06 us -> 7.91 us  [swap_cores(): lax.ppermute(x, 'kv', [(i, i ^ 1) for i in range(lax.axis_size('kv'))])]
    pallas_call x1 -> x2, Pallas kernels: 15.3 us -> 16.7 us  [the longest x1 11.3 us: cell(): pl.pallas_call(cell_kernel, out_shape=(jax.ShapeDtypeStruct((chips, rows,...]
    ppermute x3, starting transfers between devices: 4.66 us -> 3.44 us  [passed_on(): lax.ppermute(weight, 'tp', ring(tp, step))]
    ppermute x3, waiting for transfers between devices: 10.1 us -> 9.19 us  [passed_on(): lax.ppermute(weight, 'tp', ring(tp, step))]
  transfers between devices with their start and end apart: 8 -> 9, of which waited for: 4 -> 3; matrix products, arithmetic and copies ran while one was open for 0% -> 0% of each run, Pallas kernels for 0% -> 9%
where the time goes in v3:
time: 61 us; the launch traced here: 60.7 us
  starting transfers between devices  27.1 us (44%)
  Pallas kernels  17.9 us (29%)
  waiting for transfers between devices  14.1 us (23%)
  local copies, waits for them, and re-layouts  0.86 us (1%)
  between operations  0.69 us (1%)
    all_to_all x1, starting transfers between devices, project_out(): lax.all_to_all(sent.reshape(chips * tp, rows, depth), ('kv', 'tp'), 0, 0,...  12 us
    pallas_call x1, Pallas kernels, cell(): pl.pallas_call(cell_kernel, out_shape=(jax.ShapeDtypeStruct((chips, rows,...  11.3 us
    ppermute x3, waiting for transfers between devices, passed_on(): lax.ppermute(weight, 'tp', ring(tp, step))  9.19 us
    ppermute x4, starting transfers between devices, swap_cores(): lax.ppermute(x, 'kv', [(i, i ^ 1) for i in range(lax.axis_size('kv'))])  7.91 us
    pallas_call x1, Pallas kernels, cell(): pl.pallas_call(keep_kernel, out_shape=(jax.ShapeDtypeStruct(state_c.shape...  5.38 us
    all_to_all x1, waiting for transfers between devices, project_out(): lax.all_to_all(mixed.reshape(2 * tp, chips * rows, columns), ('kv', 'tp')...  3.97 us
    all_to_all x1, starting transfers between devices, project_out(): lax.all_to_all(mixed.reshape(2 * tp, chips * rows, columns), ('kv', 'tp')...  3.78 us
    ppermute x3, starting transfers between devices, passed_on(): lax.ppermute(weight, 'tp', ring(tp, step))  3.44 us
  transfers between devices with their start and end apart: 9, of which 3 were waited for; matrix products, arithmetic and copies ran while one was open for 0% of the time, Pallas kernels for 9%

profile of v3, /device:TPU:1, one launch (start us, length us, event | category | flops | bytes accessed | tf_op | source)
XLA Modules:
  0.0 60.7 jit_solution(2629865846780402226)
XLA Ops:
  0.6 0.0 copy-start
  0.6 11.3 %shard_map.216 = (bf16[16,64,512]{2,1,0:T(8,128)(2,1)}, bf16[64,512]{1,0:T(8,128)(2,1)}, bf16[64,512]{1,0:T(8,128)(2,1)}, f32[32,64]{1,0:T(8,128)}) custom-call(s32[16]{0:T(128)} %accepted.3, bf16[16,4,4096]{2,1,0:T(4,128)(2,1)} %tokens.1, bf16[4096]{0:T(1024)(128)(2,1)} %norm_gain.1, bf16[4096,512]{1,0:T(8,128)(2,1)} %query_weight.1, ...), custom_call_target="tpu_custom_call" | custom-call | flops 1073741824 | bytes 23068672 | tf_op jit(solution)/shard_map/pallas_call | solution.py:445
  11.9 12.0 %all-to-all-start = ((bf16[64,16,512]{2,1,0:T(8,128)(2,1)}), bf16[64,16,512]{2,1,0:T(8,128)(2,1)S(1)}, u32[]{:S(2)}, u32[]{:S(2)}) async-start(bf16[64,16,512]{2,1,0:T(8,128)(2,1)} %bitcast.14), calls=%async_computation | async-start | bytes 2097152 | tf_op jit(solution)/shard_map/all_to_all | solution.py:64
  23.9 0.0 copy-done
  23.9 2.3 %collective-permute-start.2 = (bf16[512,128]{1,0:T(8,128)(2,1)S(1)}, bf16[512,128]{1,0:T(8,128)(2,1)S(1)}, u32[]{:S(2)}, u32[]{:S(2)}) collective-permute-start(bf16[512,128]{1,0:T(8,128)(2,1)S(1)} %copy-done), channel_id=1, source_target_pairs={{0,3},{1,0},{2,1},{3,2},{4,7},{5,4},{6,5},{7,6},{8,11},{9,8},{10,9... | collective-permute-start | bytes 393224 | tf_op jit(solution)/shard_map/ppermute | solution.py:23
  26.2 0.6 collective-permute-start.1
  26.8 0.6 collective-permute-start
  27.4 2.1 %collective-permute-start.3 = (bf16[512,128]{1,0:T(8,128)(2,1)S(1)}, bf16[512,128]{1,0:T(8,128)(2,1)S(1)}, u32[]{:S(2)}, u32[]{:S(2)}) collective-permute-start(bf16[512,128]{1,0:T(8,128)(2,1)S(1)} %copy-done), channel_id=1, source_target_pairs={{0,4},{4,0},{8,12},{12,8},{16,20},{20,16},{24,28},{28,24},{32,36},... | collective-permute-start | bytes 393224 | tf_op jit(solution)/shard_map/ppermute | solution.py:18
  29.4 9.2 %collective-permute-done.2.refs_3_ = bf16[512,128]{1,0:T(8,128)(2,1)S(1)} collective-permute-done((bf16[512,128]{1,0:T(8,128)(2,1)S(1)}, bf16[512,128]{1,0:T(8,128)(2,1)S(1)}, u32[]{:S(2)}, u32[]{:S(2)}) %collective-permute-start.2) | collective-permute-done | bytes 131104 | tf_op jit(solution)/shard_map/ppermute | solution.py:23
  38.6 3.2 %collective-permute-start.6 = (bf16[512,128]{1,0:T(8,128)(2,1)S(1)}, bf16[512,128]{1,0:T(8,128)(2,1)S(1)}, u32[]{:S(2)}, u32[]{:S(2)}) collective-permute-start(bf16[512,128]{1,0:T(8,128)(2,1)S(1)} %collective-permute-done.2.refs_3_), channel_id=1, source_target_pairs={{0,4},{4,0},{8,12},{12,8},{16,20},{20,16},{24,28},{28,24},{32,36},... | collective-permute-start | bytes 393224 | tf_op jit(solution)/shard_map/ppermute | solution.py:18
  41.8 0.0 collective-permute-done.1.refs_2_
  41.8 1.5 %collective-permute-start.5 = (bf16[512,128]{1,0:T(8,128)(2,1)S(1)}, bf16[512,128]{1,0:T(8,128)(2,1)S(1)}, u32[]{:S(2)}, u32[]{:S(2)}) collective-permute-start(bf16[512,128]{1,0:T(8,128)(2,1)S(1)} %collective-permute-done.1.refs_2_), channel_id=1, source_target_pairs={{0,4},{4,0},{8,12},{12,8},{16,20},{20,16},{24,28},{28,24},{32,36},... | collective-permute-start | bytes 393224 | tf_op jit(solution)/shard_map/ppermute | solution.py:18
  43.3 0.0 collective-permute-done.refs_1_
  43.4 1.1 %collective-permute-start.4 = (bf16[512,128]{1,0:T(8,128)(2,1)S(1)}, bf16[512,128]{1,0:T(8,128)(2,1)S(1)}, u32[]{:S(2)}, u32[]{:S(2)}) collective-permute-start(bf16[512,128]{1,0:T(8,128)(2,1)S(1)} %collective-permute-done.refs_1_), channel_id=1, source_target_pairs={{0,4},{4,0},{8,12},{12,8},{16,20},{20,16},{24,28},{28,24},{32,36},... | collective-permute-start | bytes 393224 | tf_op jit(solution)/shard_map/ppermute | solution.py:18
  44.5 0.0 collective-permute-done.3.refs_4_
  44.5 0.0 collective-permute-done.6.refs_7_
  44.5 0.0 collective-permute-done.5.refs_6_
  44.5 1.0 %collective-permute-done.4.refs_5_ = bf16[512,128]{1,0:T(8,128)(2,1)S(1)} collective-permute-done((bf16[512,128]{1,0:T(8,128)(2,1)S(1)}, bf16[512,128]{1,0:T(8,128)(2,1)S(1)}, u32[]{:S(2)}, u32[]{:S(2)}) %collective-permute-start.4) | collective-permute-done | bytes 131104 | tf_op jit(solution)/shard_map/ppermute | solution.py:18
  45.4 0.0 all-to-all-done
  45.4 1.2 %shard_map.217 = bf16[2,4,256,128]{3,2,1,0:T(8,128)(2,1)} custom-call(bf16[16,4,16,512]{3,2,1,0:T(8,128)(2,1)S(1)} %bitcast.12, bf16[512,128]{1,0:T(8,128)(2,1)S(1)} %copy-done, bf16[512,128]{1,0:T(8,128)(2,1)S(1)} %collective-permute-done.refs_1_, bf16[512,128]{1,0:T(8,128)(2,1)S(1)} %collective-permute-done.1.refs_2_, ...), custom_call_target="tpu_custom_call" | custom-call | flops 268435456 | bytes 3145728 | tf_op jit(solution)/shard_map/pallas_call | solution.py:69
  46.7 3.8 %all-to-all-start.1 = ((bf16[8,256,128]{2,1,0:T(8,128)(2,1)}), bf16[8,256,128]{2,1,0:T(8,128)(2,1)S(1)}, u32[]{:S(2)}, u32[]{:S(2)}) async-start(bf16[8,256,128]{2,1,0:T(8,128)(2,1)} %bitcast.5), calls=%async_computation.1 | async-start | bytes 1048576 | tf_op jit(solution)/shard_map/all_to_all | solution.py:79
  50.5 5.4 %shard_map.218 = (f32[16,4,128,128]{3,2,1,0:T(8,128)}, f32[16,4,128]{2,1,0:T(4,128)}, f32[4,16]{1,0:T(4,128)}, bf16[16,4,4,128]{3,2,1,0:T(4,128)(2,1)}, bf16[16,...) custom-call(s32[16]{0:T(128)} %accepted.3, f32[16,4,128,128]{3,2,1,0:T(8,128)} %state_c.3, f32[16,4,128]{2,1,0:T(4,128)} %state_n.3, ...), custom_call_target="tpu_custom_call" | custom-call | flops 134217728 | bytes 9437184 | tf_op jit(solution)/shard_map/pallas_call | solution.py:482
  55.9 4.0 %all-to-all-done.1 = bf16[8,256,128]{2,1,0:T(8,128)(2,1)S(1)} async-done(((bf16[8,256,128]{2,1,0:T(8,128)(2,1)}), bf16[8,256,128]{2,1,0:T(8,128)(2,1)S(1)}, u32[]{:S(2)}, u32[]{:S(2)}) %all-to-all-start.1) | async-done | bytes 524320 | tf_op jit(solution)/shard_map/all_to_all | solution.py:79
  59.8 0.9 %copy.24 = bf16[2,4,16,16,128]{4,3,1,0,2:T(8,128)(2,1)} copy(bf16[2,4,16,16,128]{4,3,2,1,0:T(8,128)(2,1)S(1)} %bitcast.13) | data formatting | bytes 1048576 | tf_op jit(solution)/shard_map/reshape | solution.py:82
Async XLA Ops:
  0.6 23.3 %copy-start = (bf16[512,128]{1,0:T(8,128)(2,1)S(1)}, bf16[512,128]{1,0:T(8,128)(2,1)}, u32[]{:S(2)}) copy-start(bf16[512,128]{1,0:T(8,128)(2,1)} %refs_0_.1) | copy-start | bytes 393220
  11.9 33.5 %all-to-all-start = ((bf16[64,16,512]{2,1,0:T(8,128)(2,1)}), bf16[64,16,512]{2,1,0:T(8,128)(2,1)S(1)}, u32[]{:S(2)}, u32[]{:S(2)}) async-start(bf16[64,16,512]{2,1,0:T(8,128)(2,1)} %bitcast.14), calls=%async_computation | async-start | bytes 2097152 | tf_op jit(solution)/shard_map/all_to_all | solution.py:64
  23.9 14.7 %collective-permute-start.2 = (bf16[512,128]{1,0:T(8,128)(2,1)S(1)}, bf16[512,128]{1,0:T(8,128)(2,1)S(1)}, u32[]{:S(2)}, u32[]{:S(2)}) collective-permute-start(bf16[512,128]{1,0:T(8,128)(2,1)S(1)} %copy-done), channel_id=1, source_target_pairs={{0,3},{1,0},{2,1},{3,2},{4,7},{5,4},{6,5},{7,6},{8,11},{9,8},{10,9... | collective-permute-start | bytes 393224 | tf_op jit(solution)/shard_map/ppermute | solution.py:23
  26.2 15.6 %collective-permute-start.1 = (bf16[512,128]{1,0:T(8,128)(2,1)S(1)}, bf16[512,128]{1,0:T(8,128)(2,1)S(1)}, u32[]{:S(2)}, u32[]{:S(2)}) collective-permute-start(bf16[512,128]{1,0:T(8,128)(2,1)S(1)} %copy-done), channel_id=1, source_target_pairs={{0,2},{1,3},{2,0},{3,1},{4,6},{5,7},{6,4},{7,5},{8,10},{9,11},{10,... | collective-permute-start | bytes 393224 | tf_op jit(solution)/shard_map/ppermute | solution.py:23
  26.8 16.6 %collective-permute-start = (bf16[512,128]{1,0:T(8,128)(2,1)S(1)}, bf16[512,128]{1,0:T(8,128)(2,1)S(1)}, u32[]{:S(2)}, u32[]{:S(2)}) collective-permute-start(bf16[512,128]{1,0:T(8,128)(2,1)S(1)} %copy-done), channel_id=1, source_target_pairs={{0,1},{1,2},{2,3},{3,0},{4,5},{5,6},{6,7},{7,4},{8,9},{9,10},{10,1... | collective-permute-start | bytes 393224 | tf_op jit(solution)/shard_map/ppermute | solution.py:23
  27.4 17.1 %collective-permute-start.3 = (bf16[512,128]{1,0:T(8,128)(2,1)S(1)}, bf16[512,128]{1,0:T(8,128)(2,1)S(1)}, u32[]{:S(2)}, u32[]{:S(2)}) collective-permute-start(bf16[512,128]{1,0:T(8,128)(2,1)S(1)} %copy-done), channel_id=1, source_target_pairs={{0,4},{4,0},{8,12},{12,8},{16,20},{20,16},{24,28},{28,24},{32,36},... | collective-permute-start | bytes 393224 | tf_op jit(solution)/shard_map/ppermute | solution.py:18
  38.6 5.8 %collective-permute-start.6 = (bf16[512,128]{1,0:T(8,128)(2,1)S(1)}, bf16[512,128]{1,0:T(8,128)(2,1)S(1)}, u32[]{:S(2)}, u32[]{:S(2)}) collective-permute-start(bf16[512,128]{1,0:T(8,128)(2,1)S(1)} %collective-permute-done.2.refs_3_), channel_id=1, source_target_pairs={{0,4},{4,0},{8,12},{12,8},{16,20},{20,16},{24,28},{28,24},{32,36},... | collective-permute-start | bytes 393224 | tf_op jit(solution)/shard_map/ppermute | solution.py:18
  41.8 2.6 %collective-permute-start.5 = (bf16[512,128]{1,0:T(8,128)(2,1)S(1)}, bf16[512,128]{1,0:T(8,128)(2,1)S(1)}, u32[]{:S(2)}, u32[]{:S(2)}) collective-permute-start(bf16[512,128]{1,0:T(8,128)(2,1)S(1)} %collective-permute-done.1.refs_2_), channel_id=1, source_target_pairs={{0,4},{4,0},{8,12},{12,8},{16,20},{20,16},{24,28},{28,24},{32,36},... | collective-permute-start | bytes 393224 | tf_op jit(solution)/shard_map/ppermute | solution.py:18
  43.4 2.1 %collective-permute-start.4 = (bf16[512,128]{1,0:T(8,128)(2,1)S(1)}, bf16[512,128]{1,0:T(8,128)(2,1)S(1)}, u32[]{:S(2)}, u32[]{:S(2)}) collective-permute-start(bf16[512,128]{1,0:T(8,128)(2,1)S(1)} %collective-permute-done.refs_1_), channel_id=1, source_target_pairs={{0,4},{4,0},{8,12},{12,8},{16,20},{20,16},{24,28},{28,24},{32,36},... | collective-permute-start | bytes 393224 | tf_op jit(solution)/shard_map/ppermute | solution.py:18
  46.7 13.1 %all-to-all-start.1 = ((bf16[8,256,128]{2,1,0:T(8,128)(2,1)}), bf16[8,256,128]{2,1,0:T(8,128)(2,1)S(1)}, u32[]{:S(2)}, u32[]{:S(2)}) async-start(bf16[8,256,128]{2,1,0:T(8,128)(2,1)} %bitcast.5), calls=%async_computation.1 | async-start | bytes 1048576 | tf_op jit(solution)/shard_map/all_to_all | solution.py:79

commit v4 on v3

--- a/solution.py
+++ b/solution.py
@@ -203,6 +203,9 @@
     recall_v,
     hidden_v,
     gated_v,
+    keys_v,
+    values_v,
+    gates_v,
     sems,
     out_sems,
 ):
@@ -263,7 +266,9 @@
     cumul = exact_dot(jnp.where(causal, 1.0, 0.0), log_sigmoid(gates), (1, 0))
     gates_t = gates.T
     cumul_t = cumul.T
-    gates_out[...] = gates_t[: 2 * heads_total]
+    gates_v[...] = gates_t[: 2 * heads_total]
+    sends = [pltpu.make_async_copy(gates_v, gates_out, out_sems.at[0])]
+    sends[0].start()
 
     arrive(replay_in)
     stable, shrink, weights = replay(accepted_s, state_m_v, prev_gates_v, across)
@@ -301,9 +306,13 @@
             recall_v[pair, cols] = jnp.where(upper, found[:, :size], found[:, size:])
 
     new_keys = project(1)
-    keys_out[...] = new_keys
+    keys_v[...] = new_keys
+    sends.append(pltpu.make_async_copy(keys_v, keys_out, out_sems.at[1]))
+    sends[1].start()
     new_values = project(2)
-    values_out[...] = new_values
+    values_v[...] = new_values
+    sends.append(pltpu.make_async_copy(values_v, values_out, out_sems.at[2]))
+    sends[2].start()
     for h in range(heads):
         cols = slice(h * size, (h + 1) * size)
         query, key, value = queries[:, cols], new_keys[:, cols], new_values[:, cols]
@@ -338,12 +347,10 @@
     gated_v[...] = (
         hidden_v[...] * head_scale * jax.nn.sigmoid(outgate.astype(f32))
     ).astype(bf16)
-    sends = [
-        pltpu.make_async_copy(gated_v, gated_out.at[chip], out_sems.at[chip])
-        for chip in range(gated_out.shape[0])
-    ]
-    for copy in sends:
+    for chip in range(gated_out.shape[0]):
+        copy = pltpu.make_async_copy(gated_v, gated_out.at[chip], out_sems.at[3 + chip])
         copy.start()
+        sends.append(copy)
     arrive(sends)
 
 
@@ -451,7 +458,7 @@
             jax.ShapeDtypeStruct((gate_weight.shape[1], rows), f32),
         ),
         in_specs=[anywhere] * 16,
-        out_specs=[anywhere] + [here] * 3,
+        out_specs=[anywhere] * 4,
         scratch_shapes=[
             pltpu.SMEM(accepted.shape, jnp.int32),
             pltpu.VMEM(tokens.shape, bf16),
@@ -471,8 +478,11 @@
             pltpu.VMEM((rows, columns), f32),
             pltpu.VMEM((rows, columns), f32),
             pltpu.VMEM((rows, columns), bf16),
+            pltpu.VMEM((rows, columns), bf16),
+            pltpu.VMEM((rows, columns), bf16),
+            pltpu.VMEM((gate_weight.shape[1], rows), f32),
             pltpu.SemaphoreType.DMA((11 + 16 + heads,)),
-            pltpu.SemaphoreType.DMA((chips,)),
+            pltpu.SemaphoreType.DMA((3 + chips,)),
         ],
         compiler_params=pltpu.CompilerParams(vmem_limit_bytes=62 * 1024 * 1024),
         cost_estimate=pl.CostEstimate(

time: 61 us -> 60.4 us (level)
    pallas_call x1, Pallas kernels: 11.3 us -> 10.6 us  [cell(): pl.pallas_call(cell_kernel, out_shape=(jax.ShapeDtypeStruct((chips, rows,...]
where the time goes in v4:
time: 60.4 us; the launch traced here: 60 us
  starting transfers between devices  27.1 us (45%)
  Pallas kernels  17.3 us (29%)
  waiting for transfers between devices  14.1 us (23%)
  local copies, waits for them, and re-layouts  0.86 us (1%)
  between operations  0.69 us (1%)
    all_to_all x1, starting transfers between devices, project_out(): lax.all_to_all(sent.reshape(chips * tp, rows, depth), ('kv', 'tp'), 0, 0,...  12 us
    pallas_call x1, Pallas kernels, cell(): pl.pallas_call(cell_kernel, out_shape=(jax.ShapeDtypeStruct((chips, rows,...  10.6 us
    ppermute x3, waiting for transfers between devices, passed_on(): lax.ppermute(weight, 'tp', ring(tp, step))  9.2 us
    ppermute x4, starting transfers between devices, swap_cores(): lax.ppermute(x, 'kv', [(i, i ^ 1) for i in range(lax.axis_size('kv'))])  7.9 us
    pallas_call x1, Pallas kernels, cell(): pl.pallas_call(keep_kernel, out_shape=(jax.ShapeDtypeStruct(state_c.shape...  5.39 us
    all_to_all x1, waiting for transfers between devices, project_out(): lax.all_to_all(mixed.reshape(2 * tp, chips * rows, columns), ('kv', 'tp')...  3.96 us
    all_to_all x1, starting transfers between devices, project_out(): lax.all_to_all(mixed.reshape(2 * tp, chips * rows, columns), ('kv', 'tp')...  3.78 us
    ppermute x3, starting transfers between devices, passed_on(): lax.ppermute(weight, 'tp', ring(tp, step))  3.44 us
  transfers between devices with their start and end apart: 9, of which 3 were waited for; matrix products, arithmetic and copies ran while one was open for 0% of the time, Pallas kernels for 9%

profile of v4, /device:TPU:1, one launch (start us, length us, event | category | flops | bytes accessed | tf_op | source)
XLA Modules:
  0.0 60.0 jit_solution(15394786436893226933)
XLA Ops:
  0.6 0.0 copy-start
  0.6 10.6 %shard_map.216 = (bf16[16,64,512]{2,1,0:T(8,128)(2,1)}, bf16[64,512]{1,0:T(8,128)(2,1)}, bf16[64,512]{1,0:T(8,128)(2,1)}, f32[32,64]{1,0:T(8,128)}) custom-call(s32[16]{0:T(128)} %accepted.3, bf16[16,4,4096]{2,1,0:T(4,128)(2,1)} %tokens.1, bf16[4096]{0:T(1024)(128)(2,1)} %norm_gain.1, bf16[4096,512]{1,0:T(8,128)(2,1)} %query_weight.1, ...), custom_call_target="tpu_custom_call" | custom-call | flops 1073741824 | bytes 23068672 | tf_op jit(solution)/shard_map/pallas_call | solution.py:452
  11.3 12.0 %all-to-all-start = ((bf16[64,16,512]{2,1,0:T(8,128)(2,1)}), bf16[64,16,512]{2,1,0:T(8,128)(2,1)S(1)}, u32[]{:S(2)}, u32[]{:S(2)}) async-start(bf16[64,16,512]{2,1,0:T(8,128)(2,1)} %bitcast.14), calls=%async_computation | async-start | bytes 2097152 | tf_op jit(solution)/shard_map/all_to_all | solution.py:64
  23.3 0.0 copy-done
  23.3 2.3 %collective-permute-start.2 = (bf16[512,128]{1,0:T(8,128)(2,1)S(1)}, bf16[512,128]{1,0:T(8,128)(2,1)S(1)}, u32[]{:S(2)}, u32[]{:S(2)}) collective-permute-start(bf16[512,128]{1,0:T(8,128)(2,1)S(1)} %copy-done), channel_id=1, source_target_pairs={{0,3},{1,0},{2,1},{3,2},{4,7},{5,4},{6,5},{7,6},{8,11},{9,8},{10,9... | collective-permute-start | bytes 393224 | tf_op jit(solution)/shard_map/ppermute | solution.py:23
  25.6 0.6 collective-permute-start.1
  26.1 0.6 collective-permute-start
  26.7 2.1 %collective-permute-start.3 = (bf16[512,128]{1,0:T(8,128)(2,1)S(1)}, bf16[512,128]{1,0:T(8,128)(2,1)S(1)}, u32[]{:S(2)}, u32[]{:S(2)}) collective-permute-start(bf16[512,128]{1,0:T(8,128)(2,1)S(1)} %copy-done), channel_id=1, source_target_pairs={{0,4},{4,0},{8,12},{12,8},{16,20},{20,16},{24,28},{28,24},{32,36},... | collective-permute-start | bytes 393224 | tf_op jit(solution)/shard_map/ppermute | solution.py:18
  28.8 9.2 %collective-permute-done.2.refs_3_ = bf16[512,128]{1,0:T(8,128)(2,1)S(1)} collective-permute-done((bf16[512,128]{1,0:T(8,128)(2,1)S(1)}, bf16[512,128]{1,0:T(8,128)(2,1)S(1)}, u32[]{:S(2)}, u32[]{:S(2)}) %collective-permute-start.2) | collective-permute-done | bytes 131104 | tf_op jit(solution)/shard_map/ppermute | solution.py:23
  38.0 3.2 %collective-permute-start.6 = (bf16[512,128]{1,0:T(8,128)(2,1)S(1)}, bf16[512,128]{1,0:T(8,128)(2,1)S(1)}, u32[]{:S(2)}, u32[]{:S(2)}) collective-permute-start(bf16[512,128]{1,0:T(8,128)(2,1)S(1)} %collective-permute-done.2.refs_3_), channel_id=1, source_target_pairs={{0,4},{4,0},{8,12},{12,8},{16,20},{20,16},{24,28},{28,24},{32,36},... | collective-permute-start | bytes 393224 | tf_op jit(solution)/shard_map/ppermute | solution.py:18
  41.2 0.0 collective-permute-done.1.refs_2_
  41.2 1.5 %collective-permute-start.5 = (bf16[512,128]{1,0:T(8,128)(2,1)S(1)}, bf16[512,128]{1,0:T(8,128)(2,1)S(1)}, u32[]{:S(2)}, u32[]{:S(2)}) collective-permute-start(bf16[512,128]{1,0:T(8,128)(2,1)S(1)} %collective-permute-done.1.refs_2_), channel_id=1, source_target_pairs={{0,4},{4,0},{8,12},{12,8},{16,20},{20,16},{24,28},{28,24},{32,36},... | collective-permute-start | bytes 393224 | tf_op jit(solution)/shard_map/ppermute | solution.py:18
  42.7 0.0 collective-permute-done.refs_1_
  42.7 1.1 %collective-permute-start.4 = (bf16[512,128]{1,0:T(8,128)(2,1)S(1)}, bf16[512,128]{1,0:T(8,128)(2,1)S(1)}, u32[]{:S(2)}, u32[]{:S(2)}) collective-permute-start(bf16[512,128]{1,0:T(8,128)(2,1)S(1)} %collective-permute-done.refs_1_), channel_id=1, source_target_pairs={{0,4},{4,0},{8,12},{12,8},{16,20},{20,16},{24,28},{28,24},{32,36},... | collective-permute-start | bytes 393224 | tf_op jit(solution)/shard_map/ppermute | solution.py:18
  43.8 0.0 collective-permute-done.3.refs_4_
  43.8 0.0 collective-permute-done.6.refs_7_
  43.8 0.0 collective-permute-done.5.refs_6_
  43.8 1.0 %collective-permute-done.4.refs_5_ = bf16[512,128]{1,0:T(8,128)(2,1)S(1)} collective-permute-done((bf16[512,128]{1,0:T(8,128)(2,1)S(1)}, bf16[512,128]{1,0:T(8,128)(2,1)S(1)}, u32[]{:S(2)}, u32[]{:S(2)}) %collective-permute-start.4) | collective-permute-done | bytes 131104 | tf_op jit(solution)/shard_map/ppermute | solution.py:18
  44.8 0.0 all-to-all-done
  44.8 1.2 %shard_map.217 = bf16[2,4,256,128]{3,2,1,0:T(8,128)(2,1)} custom-call(bf16[16,4,16,512]{3,2,1,0:T(8,128)(2,1)S(1)} %bitcast.12, bf16[512,128]{1,0:T(8,128)(2,1)S(1)} %copy-done, bf16[512,128]{1,0:T(8,128)(2,1)S(1)} %collective-permute-done.refs_1_, bf16[512,128]{1,0:T(8,128)(2,1)S(1)} %collective-permute-done.1.refs_2_, ...), custom_call_target="tpu_custom_call" | custom-call | flops 268435456 | bytes 3145728 | tf_op jit(solution)/shard_map/pallas_call | solution.py:69
  46.0 3.8 %all-to-all-start.1 = ((bf16[8,256,128]{2,1,0:T(8,128)(2,1)}), bf16[8,256,128]{2,1,0:T(8,128)(2,1)S(1)}, u32[]{:S(2)}, u32[]{:S(2)}) async-start(bf16[8,256,128]{2,1,0:T(8,128)(2,1)} %bitcast.5), calls=%async_computation.1 | async-start | bytes 1048576 | tf_op jit(solution)/shard_map/all_to_all | solution.py:79
  49.8 5.4 %shard_map.218 = (f32[16,4,128,128]{3,2,1,0:T(8,128)}, f32[16,4,128]{2,1,0:T(4,128)}, f32[4,16]{1,0:T(4,128)}, bf16[16,4,4,128]{3,2,1,0:T(4,128)(2,1)}, bf16[16,...) custom-call(s32[16]{0:T(128)} %accepted.3, f32[16,4,128,128]{3,2,1,0:T(8,128)} %state_c.3, f32[16,4,128]{2,1,0:T(4,128)} %state_n.3, ...), custom_call_target="tpu_custom_call" | custom-call | flops 134217728 | bytes 9437184 | tf_op jit(solution)/shard_map/pallas_call | solution.py:492
  55.2 4.0 %all-to-all-done.1 = bf16[8,256,128]{2,1,0:T(8,128)(2,1)S(1)} async-done(((bf16[8,256,128]{2,1,0:T(8,128)(2,1)}), bf16[8,256,128]{2,1,0:T(8,128)(2,1)S(1)}, u32[]{:S(2)}, u32[]{:S(2)}) %all-to-all-start.1) | async-done | bytes 524320 | tf_op jit(solution)/shard_map/all_to_all | solution.py:79
  59.2 0.9 %copy.24 = bf16[2,4,16,16,128]{4,3,1,0,2:T(8,128)(2,1)} copy(bf16[2,4,16,16,128]{4,3,2,1,0:T(8,128)(2,1)S(1)} %bitcast.13) | data formatting | bytes 1048576 | tf_op jit(solution)/shard_map/reshape | solution.py:82
Async XLA Ops:
  0.6 22.6 %copy-start = (bf16[512,128]{1,0:T(8,128)(2,1)S(1)}, bf16[512,128]{1,0:T(8,128)(2,1)}, u32[]{:S(2)}) copy-start(bf16[512,128]{1,0:T(8,128)(2,1)} %refs_0_.1) | copy-start | bytes 393220
  11.3 33.5 %all-to-all-start = ((bf16[64,16,512]{2,1,0:T(8,128)(2,1)}), bf16[64,16,512]{2,1,0:T(8,128)(2,1)S(1)}, u32[]{:S(2)}, u32[]{:S(2)}) async-start(bf16[64,16,512]{2,1,0:T(8,128)(2,1)} %bitcast.14), calls=%async_computation | async-start | bytes 2097152 | tf_op jit(solution)/shard_map/all_to_all | solution.py:64
  23.3 14.7 %collective-permute-start.2 = (bf16[512,128]{1,0:T(8,128)(2,1)S(1)}, bf16[512,128]{1,0:T(8,128)(2,1)S(1)}, u32[]{:S(2)}, u32[]{:S(2)}) collective-permute-start(bf16[512,128]{1,0:T(8,128)(2,1)S(1)} %copy-done), channel_id=1, source_target_pairs={{0,3},{1,0},{2,1},{3,2},{4,7},{5,4},{6,5},{7,6},{8,11},{9,8},{10,9... | collective-permute-start | bytes 393224 | tf_op jit(solution)/shard_map/ppermute | solution.py:23
  25.6 15.6 %collective-permute-start.1 = (bf16[512,128]{1,0:T(8,128)(2,1)S(1)}, bf16[512,128]{1,0:T(8,128)(2,1)S(1)}, u32[]{:S(2)}, u32[]{:S(2)}) collective-permute-start(bf16[512,128]{1,0:T(8,128)(2,1)S(1)} %copy-done), channel_id=1, source_target_pairs={{0,2},{1,3},{2,0},{3,1},{4,6},{5,7},{6,4},{7,5},{8,10},{9,11},{10,... | collective-permute-start | bytes 393224 | tf_op jit(solution)/shard_map/ppermute | solution.py:23
  26.1 16.6 %collective-permute-start = (bf16[512,128]{1,0:T(8,128)(2,1)S(1)}, bf16[512,128]{1,0:T(8,128)(2,1)S(1)}, u32[]{:S(2)}, u32[]{:S(2)}) collective-permute-start(bf16[512,128]{1,0:T(8,128)(2,1)S(1)} %copy-done), channel_id=1, source_target_pairs={{0,1},{1,2},{2,3},{3,0},{4,5},{5,6},{6,7},{7,4},{8,9},{9,10},{10,1... | collective-permute-start | bytes 393224 | tf_op jit(solution)/shard_map/ppermute | solution.py:23
  26.7 17.1 %collective-permute-start.3 = (bf16[512,128]{1,0:T(8,128)(2,1)S(1)}, bf16[512,128]{1,0:T(8,128)(2,1)S(1)}, u32[]{:S(2)}, u32[]{:S(2)}) collective-permute-start(bf16[512,128]{1,0:T(8,128)(2,1)S(1)} %copy-done), channel_id=1, source_target_pairs={{0,4},{4,0},{8,12},{12,8},{16,20},{20,16},{24,28},{28,24},{32,36},... | collective-permute-start | bytes 393224 | tf_op jit(solution)/shard_map/ppermute | solution.py:18
  38.0 5.8 %collective-permute-start.6 = (bf16[512,128]{1,0:T(8,128)(2,1)S(1)}, bf16[512,128]{1,0:T(8,128)(2,1)S(1)}, u32[]{:S(2)}, u32[]{:S(2)}) collective-permute-start(bf16[512,128]{1,0:T(8,128)(2,1)S(1)} %collective-permute-done.2.refs_3_), channel_id=1, source_target_pairs={{0,4},{4,0},{8,12},{12,8},{16,20},{20,16},{24,28},{28,24},{32,36},... | collective-permute-start | bytes 393224 | tf_op jit(solution)/shard_map/ppermute | solution.py:18
  41.2 2.6 %collective-permute-start.5 = (bf16[512,128]{1,0:T(8,128)(2,1)S(1)}, bf16[512,128]{1,0:T(8,128)(2,1)S(1)}, u32[]{:S(2)}, u32[]{:S(2)}) collective-permute-start(bf16[512,128]{1,0:T(8,128)(2,1)S(1)} %collective-permute-done.1.refs_2_), channel_id=1, source_target_pairs={{0,4},{4,0},{8,12},{12,8},{16,20},{20,16},{24,28},{28,24},{32,36},... | collective-permute-start | bytes 393224 | tf_op jit(solution)/shard_map/ppermute | solution.py:18
  42.7 2.1 %collective-permute-start.4 = (bf16[512,128]{1,0:T(8,128)(2,1)S(1)}, bf16[512,128]{1,0:T(8,128)(2,1)S(1)}, u32[]{:S(2)}, u32[]{:S(2)}) collective-permute-start(bf16[512,128]{1,0:T(8,128)(2,1)S(1)} %collective-permute-done.refs_1_), channel_id=1, source_target_pairs={{0,4},{4,0},{8,12},{12,8},{16,20},{20,16},{24,28},{28,24},{32,36},... | collective-permute-start | bytes 393224 | tf_op jit(solution)/shard_map/ppermute | solution.py:18
  46.0 13.1 %all-to-all-start.1 = ((bf16[8,256,128]{2,1,0:T(8,128)(2,1)}), bf16[8,256,128]{2,1,0:T(8,128)(2,1)S(1)}, u32[]{:S(2)}, u32[]{:S(2)}) async-start(bf16[8,256,128]{2,1,0:T(8,128)(2,1)} %bitcast.5), calls=%async_computation.1 | async-start | bytes 1048576 | tf_op jit(solution)/shard_map/all_to_all | solution.py:79

commit v5 on v4

--- a/solution.py
+++ b/solution.py
@@ -20,7 +20,10 @@
 
 def passed_on(weight):
     tp = lax.axis_size("tp")
-    return [weight] + [lax.ppermute(weight, "tp", ring(tp, step)) for step in range(1, tp)]
+    passed = [weight]
+    for step in range(1, tp):
+        passed.append(lax.ppermute(weight, "tp", ring(tp, step)))
+    return passed
 
 
 def mix_kernel(received, *refs):

time: 60.4 us -> 60.4 us (level)
  no operation moved by 1% of the time
where the time goes in v5:
time: 60.4 us; the launch traced here: 60 us
  starting transfers between devices  27.1 us (45%)
  Pallas kernels  17.3 us (29%)
  waiting for transfers between devices  14.1 us (23%)
  local copies, waits for them, and re-layouts  0.86 us (1%)
  between operations  0.69 us (1%)
    all_to_all x1, starting transfers between devices, project_out(): lax.all_to_all(sent.reshape(chips * tp, rows, depth), ('kv', 'tp'), 0, 0,...  12 us
    pallas_call x1, Pallas kernels, cell(): pl.pallas_call(cell_kernel, out_shape=(jax.ShapeDtypeStruct((chips, rows,...  10.6 us
    ppermute x3, waiting for transfers between devices, passed_on(): passed.append(lax.ppermute(weight, 'tp', ring(tp, step)))  9.2 us
    ppermute x4, starting transfers between devices, swap_cores(): lax.ppermute(x, 'kv', [(i, i ^ 1) for i in range(lax.axis_size('kv'))])  7.9 us
    pallas_call x1, Pallas kernels, cell(): pl.pallas_call(keep_kernel, out_shape=(jax.ShapeDtypeStruct(state_c.shape...  5.39 us
    all_to_all x1, waiting for transfers between devices, project_out(): lax.all_to_all(mixed.reshape(2 * tp, chips * rows, columns), ('kv', 'tp')...  3.96 us
    all_to_all x1, starting transfers between devices, project_out(): lax.all_to_all(mixed.reshape(2 * tp, chips * rows, columns), ('kv', 'tp')...  3.78 us
    ppermute x3, starting transfers between devices, passed_on(): passed.append(lax.ppermute(weight, 'tp', ring(tp, step)))  3.44 us
  transfers between devices with their start and end apart: 9, of which 3 were waited for; matrix products, arithmetic and copies ran while one was open for 0% of the time, Pallas kernels for 9%

profile of v5, /device:TPU:1, one launch (start us, length us, event | category | flops | bytes accessed | tf_op | source)
XLA Modules:
  0.0 60.0 jit_solution(15394786436893226933)
XLA Ops:
  0.6 0.0 copy-start
  0.6 10.6 %shard_map.216 = (bf16[16,64,512]{2,1,0:T(8,128)(2,1)}, bf16[64,512]{1,0:T(8,128)(2,1)}, bf16[64,512]{1,0:T(8,128)(2,1)}, f32[32,64]{1,0:T(8,128)}) custom-call(s32[16]{0:T(128)} %accepted.3, bf16[16,4,4096]{2,1,0:T(4,128)(2,1)} %tokens.1, bf16[4096]{0:T(1024)(128)(2,1)} %norm_gain.1, bf16[4096,512]{1,0:T(8,128)(2,1)} %query_weight.1, ...), custom_call_target="tpu_custom_call" | custom-call | flops 1073741824 | bytes 23068672 | tf_op jit(solution)/shard_map/pallas_call | solution.py:455
  11.3 12.0 %all-to-all-start = ((bf16[64,16,512]{2,1,0:T(8,128)(2,1)}), bf16[64,16,512]{2,1,0:T(8,128)(2,1)S(1)}, u32[]{:S(2)}, u32[]{:S(2)}) async-start(bf16[64,16,512]{2,1,0:T(8,128)(2,1)} %bitcast.14), calls=%async_computation | async-start | bytes 2097152 | tf_op jit(solution)/shard_map/all_to_all | solution.py:67
  23.3 0.0 copy-done
  23.3 2.3 %collective-permute-start.2 = (bf16[512,128]{1,0:T(8,128)(2,1)S(1)}, bf16[512,128]{1,0:T(8,128)(2,1)S(1)}, u32[]{:S(2)}, u32[]{:S(2)}) collective-permute-start(bf16[512,128]{1,0:T(8,128)(2,1)S(1)} %copy-done), channel_id=1, source_target_pairs={{0,3},{1,0},{2,1},{3,2},{4,7},{5,4},{6,5},{7,6},{8,11},{9,8},{10,9... | collective-permute-start | bytes 393224 | tf_op jit(solution)/shard_map/ppermute | solution.py:25
  25.6 0.6 collective-permute-start.1
  26.1 0.6 collective-permute-start
  26.7 2.1 %collective-permute-start.3 = (bf16[512,128]{1,0:T(8,128)(2,1)S(1)}, bf16[512,128]{1,0:T(8,128)(2,1)S(1)}, u32[]{:S(2)}, u32[]{:S(2)}) collective-permute-start(bf16[512,128]{1,0:T(8,128)(2,1)S(1)} %copy-done), channel_id=1, source_target_pairs={{0,4},{4,0},{8,12},{12,8},{16,20},{20,16},{24,28},{28,24},{32,36},... | collective-permute-start | bytes 393224 | tf_op jit(solution)/shard_map/ppermute | solution.py:18
  28.8 9.2 %collective-permute-done.2.refs_3_ = bf16[512,128]{1,0:T(8,128)(2,1)S(1)} collective-permute-done((bf16[512,128]{1,0:T(8,128)(2,1)S(1)}, bf16[512,128]{1,0:T(8,128)(2,1)S(1)}, u32[]{:S(2)}, u32[]{:S(2)}) %collective-permute-start.2) | collective-permute-done | bytes 131104 | tf_op jit(solution)/shard_map/ppermute | solution.py:25
  38.0 3.2 %collective-permute-start.6 = (bf16[512,128]{1,0:T(8,128)(2,1)S(1)}, bf16[512,128]{1,0:T(8,128)(2,1)S(1)}, u32[]{:S(2)}, u32[]{:S(2)}) collective-permute-start(bf16[512,128]{1,0:T(8,128)(2,1)S(1)} %collective-permute-done.2.refs_3_), channel_id=1, source_target_pairs={{0,4},{4,0},{8,12},{12,8},{16,20},{20,16},{24,28},{28,24},{32,36},... | collective-permute-start | bytes 393224 | tf_op jit(solution)/shard_map/ppermute | solution.py:18
  41.2 0.0 collective-permute-done.1.refs_2_
  41.2 1.5 %collective-permute-start.5 = (bf16[512,128]{1,0:T(8,128)(2,1)S(1)}, bf16[512,128]{1,0:T(8,128)(2,1)S(1)}, u32[]{:S(2)}, u32[]{:S(2)}) collective-permute-start(bf16[512,128]{1,0:T(8,128)(2,1)S(1)} %collective-permute-done.1.refs_2_), channel_id=1, source_target_pairs={{0,4},{4,0},{8,12},{12,8},{16,20},{20,16},{24,28},{28,24},{32,36},... | collective-permute-start | bytes 393224 | tf_op jit(solution)/shard_map/ppermute | solution.py:18
  42.7 0.0 collective-permute-done.refs_1_
  42.7 1.1 %collective-permute-start.4 = (bf16[512,128]{1,0:T(8,128)(2,1)S(1)}, bf16[512,128]{1,0:T(8,128)(2,1)S(1)}, u32[]{:S(2)}, u32[]{:S(2)}) collective-permute-start(bf16[512,128]{1,0:T(8,128)(2,1)S(1)} %collective-permute-done.refs_1_), channel_id=1, source_target_pairs={{0,4},{4,0},{8,12},{12,8},{16,20},{20,16},{24,28},{28,24},{32,36},... | collective-permute-start | bytes 393224 | tf_op jit(solution)/shard_map/ppermute | solution.py:18
  43.8 0.0 collective-permute-done.3.refs_4_
  43.8 0.0 collective-permute-done.6.refs_7_
  43.8 0.0 collective-permute-done.5.refs_6_
  43.8 1.0 %collective-permute-done.4.refs_5_ = bf16[512,128]{1,0:T(8,128)(2,1)S(1)} collective-permute-done((bf16[512,128]{1,0:T(8,128)(2,1)S(1)}, bf16[512,128]{1,0:T(8,128)(2,1)S(1)}, u32[]{:S(2)}, u32[]{:S(2)}) %collective-permute-start.4) | collective-permute-done | bytes 131104 | tf_op jit(solution)/shard_map/ppermute | solution.py:18
  44.8 0.0 all-to-all-done
  44.8 1.2 %shard_map.217 = bf16[2,4,256,128]{3,2,1,0:T(8,128)(2,1)} custom-call(bf16[16,4,16,512]{3,2,1,0:T(8,128)(2,1)S(1)} %bitcast.12, bf16[512,128]{1,0:T(8,128)(2,1)S(1)} %copy-done, bf16[512,128]{1,0:T(8,128)(2,1)S(1)} %collective-permute-done.refs_1_, bf16[512,128]{1,0:T(8,128)(2,1)S(1)} %collective-permute-done.1.refs_2_, ...), custom_call_target="tpu_custom_call" | custom-call | flops 268435456 | bytes 3145728 | tf_op jit(solution)/shard_map/pallas_call | solution.py:72
  46.0 3.8 %all-to-all-start.1 = ((bf16[8,256,128]{2,1,0:T(8,128)(2,1)}), bf16[8,256,128]{2,1,0:T(8,128)(2,1)S(1)}, u32[]{:S(2)}, u32[]{:S(2)}) async-start(bf16[8,256,128]{2,1,0:T(8,128)(2,1)} %bitcast.5), calls=%async_computation.1 | async-start | bytes 1048576 | tf_op jit(solution)/shard_map/all_to_all | solution.py:82
  49.8 5.4 %shard_map.218 = (f32[16,4,128,128]{3,2,1,0:T(8,128)}, f32[16,4,128]{2,1,0:T(4,128)}, f32[4,16]{1,0:T(4,128)}, bf16[16,4,4,128]{3,2,1,0:T(4,128)(2,1)}, bf16[16,...) custom-call(s32[16]{0:T(128)} %accepted.3, f32[16,4,128,128]{3,2,1,0:T(8,128)} %state_c.3, f32[16,4,128]{2,1,0:T(4,128)} %state_n.3, ...), custom_call_target="tpu_custom_call" | custom-call | flops 134217728 | bytes 9437184 | tf_op jit(solution)/shard_map/pallas_call | solution.py:495
  55.2 4.0 %all-to-all-done.1 = bf16[8,256,128]{2,1,0:T(8,128)(2,1)S(1)} async-done(((bf16[8,256,128]{2,1,0:T(8,128)(2,1)}), bf16[8,256,128]{2,1,0:T(8,128)(2,1)S(1)}, u32[]{:S(2)}, u32[]{:S(2)}) %all-to-all-start.1) | async-done | bytes 524320 | tf_op jit(solution)/shard_map/all_to_all | solution.py:82
  59.2 0.9 %copy.24 = bf16[2,4,16,16,128]{4,3,1,0,2:T(8,128)(2,1)} copy(bf16[2,4,16,16,128]{4,3,2,1,0:T(8,128)(2,1)S(1)} %bitcast.13) | data formatting | bytes 1048576 | tf_op jit(solution)/shard_map/reshape | solution.py:85
Async XLA Ops:
  0.6 22.6 %copy-start = (bf16[512,128]{1,0:T(8,128)(2,1)S(1)}, bf16[512,128]{1,0:T(8,128)(2,1)}, u32[]{:S(2)}) copy-start(bf16[512,128]{1,0:T(8,128)(2,1)} %refs_0_.1) | copy-start | bytes 393220
  11.3 33.5 %all-to-all-start = ((bf16[64,16,512]{2,1,0:T(8,128)(2,1)}), bf16[64,16,512]{2,1,0:T(8,128)(2,1)S(1)}, u32[]{:S(2)}, u32[]{:S(2)}) async-start(bf16[64,16,512]{2,1,0:T(8,128)(2,1)} %bitcast.14), calls=%async_computation | async-start | bytes 2097152 | tf_op jit(solution)/shard_map/all_to_all | solution.py:67
  23.3 14.7 %collective-permute-start.2 = (bf16[512,128]{1,0:T(8,128)(2,1)S(1)}, bf16[512,128]{1,0:T(8,128)(2,1)S(1)}, u32[]{:S(2)}, u32[]{:S(2)}) collective-permute-start(bf16[512,128]{1,0:T(8,128)(2,1)S(1)} %copy-done), channel_id=1, source_target_pairs={{0,3},{1,0},{2,1},{3,2},{4,7},{5,4},{6,5},{7,6},{8,11},{9,8},{10,9... | collective-permute-start | bytes 393224 | tf_op jit(solution)/shard_map/ppermute | solution.py:25
  25.6 15.6 %collective-permute-start.1 = (bf16[512,128]{1,0:T(8,128)(2,1)S(1)}, bf16[512,128]{1,0:T(8,128)(2,1)S(1)}, u32[]{:S(2)}, u32[]{:S(2)}) collective-permute-start(bf16[512,128]{1,0:T(8,128)(2,1)S(1)} %copy-done), channel_id=1, source_target_pairs={{0,2},{1,3},{2,0},{3,1},{4,6},{5,7},{6,4},{7,5},{8,10},{9,11},{10,... | collective-permute-start | bytes 393224 | tf_op jit(solution)/shard_map/ppermute | solution.py:25
  26.1 16.6 %collective-permute-start = (bf16[512,128]{1,0:T(8,128)(2,1)S(1)}, bf16[512,128]{1,0:T(8,128)(2,1)S(1)}, u32[]{:S(2)}, u32[]{:S(2)}) collective-permute-start(bf16[512,128]{1,0:T(8,128)(2,1)S(1)} %copy-done), channel_id=1, source_target_pairs={{0,1},{1,2},{2,3},{3,0},{4,5},{5,6},{6,7},{7,4},{8,9},{9,10},{10,1... | collective-permute-start | bytes 393224 | tf_op jit(solution)/shard_map/ppermute | solution.py:25
  26.7 17.1 %collective-permute-start.3 = (bf16[512,128]{1,0:T(8,128)(2,1)S(1)}, bf16[512,128]{1,0:T(8,128)(2,1)S(1)}, u32[]{:S(2)}, u32[]{:S(2)}) collective-permute-start(bf16[512,128]{1,0:T(8,128)(2,1)S(1)} %copy-done), channel_id=1, source_target_pairs={{0,4},{4,0},{8,12},{12,8},{16,20},{20,16},{24,28},{28,24},{32,36},... | collective-permute-start | bytes 393224 | tf_op jit(solution)/shard_map/ppermute | solution.py:18
  38.0 5.8 %collective-permute-start.6 = (bf16[512,128]{1,0:T(8,128)(2,1)S(1)}, bf16[512,128]{1,0:T(8,128)(2,1)S(1)}, u32[]{:S(2)}, u32[]{:S(2)}) collective-permute-start(bf16[512,128]{1,0:T(8,128)(2,1)S(1)} %collective-permute-done.2.refs_3_), channel_id=1, source_target_pairs={{0,4},{4,0},{8,12},{12,8},{16,20},{20,16},{24,28},{28,24},{32,36},... | collective-permute-start | bytes 393224 | tf_op jit(solution)/shard_map/ppermute | solution.py:18
  41.2 2.6 %collective-permute-start.5 = (bf16[512,128]{1,0:T(8,128)(2,1)S(1)}, bf16[512,128]{1,0:T(8,128)(2,1)S(1)}, u32[]{:S(2)}, u32[]{:S(2)}) collective-permute-start(bf16[512,128]{1,0:T(8,128)(2,1)S(1)} %collective-permute-done.1.refs_2_), channel_id=1, source_target_pairs={{0,4},{4,0},{8,12},{12,8},{16,20},{20,16},{24,28},{28,24},{32,36},... | collective-permute-start | bytes 393224 | tf_op jit(solution)/shard_map/ppermute | solution.py:18
  42.7 2.1 %collective-permute-start.4 = (bf16[512,128]{1,0:T(8,128)(2,1)S(1)}, bf16[512,128]{1,0:T(8,128)(2,1)S(1)}, u32[]{:S(2)}, u32[]{:S(2)}) collective-permute-start(bf16[512,128]{1,0:T(8,128)(2,1)S(1)} %collective-permute-done.refs_1_), channel_id=1, source_target_pairs={{0,4},{4,0},{8,12},{12,8},{16,20},{20,16},{24,28},{28,24},{32,36},... | collective-permute-start | bytes 393224 | tf_op jit(solution)/shard_map/ppermute | solution.py:18
  46.0 13.1 %all-to-all-start.1 = ((bf16[8,256,128]{2,1,0:T(8,128)(2,1)}), bf16[8,256,128]{2,1,0:T(8,128)(2,1)S(1)}, u32[]{:S(2)}, u32[]{:S(2)}) async-start(bf16[8,256,128]{2,1,0:T(8,128)(2,1)} %bitcast.5), calls=%async_computation.1 | async-start | bytes 1048576 | tf_op jit(solution)/shard_map/all_to_all | solution.py:82

commit v6 on v5

--- a/solution.py
+++ b/solution.py
@@ -299,13 +299,11 @@
         states_in[h].wait()
         for p in range(seqs // 2):
             stacked = [
-                jnp.concatenate(split(state_c_v[h, b]), axis=1) for b in (2 * p, 2 * p + 1)
+                state_c_v[h, b].astype(bf16) for b in (2 * p, 2 * p + 1)
             ]
             pair = slice(2 * p * props, 2 * (p + 1) * props)
             asked = query_f[pair].astype(bf16)
-            found = dot_nt(
-                jnp.concatenate([asked, asked], axis=1), jnp.concatenate(stacked, axis=0)
-            )
+            found = dot_nt(asked, jnp.concatenate(stacked, axis=0))
             recall_v[pair, cols] = jnp.where(upper, found[:, :size], found[:, size:])
 
     new_keys = project(1)

time: 60.4 us -> 59.9 us (level)
  no operation moved by 1% of the time
where the time goes in v6:
time: 59.9 us; the launch traced here: 59.6 us
  starting transfers between devices  27.1 us (45%)
  Pallas kernels  16.8 us (28%)
  waiting for transfers between devices  14.2 us (24%)
  local copies, waits for them, and re-layouts  0.86 us (1%)
  between operations  0.69 us (1%)
    all_to_all x1, starting transfers between devices, project_out(): lax.all_to_all(sent.reshape(chips * tp, rows, depth), ('kv', 'tp'), 0, 0,...  12 us
    pallas_call x1, Pallas kernels, cell(): pl.pallas_call(cell_kernel, out_shape=(jax.ShapeDtypeStruct((chips, rows,...  10.2 us
    ppermute x3, waiting for transfers between devices, passed_on(): passed.append(lax.ppermute(weight, 'tp', ring(tp, step)))  9.2 us
    ppermute x4, starting transfers between devices, swap_cores(): lax.ppermute(x, 'kv', [(i, i ^ 1) for i in range(lax.axis_size('kv'))])  7.9 us
    pallas_call x1, Pallas kernels, cell(): pl.pallas_call(keep_kernel, out_shape=(jax.ShapeDtypeStruct(state_c.shape...  5.38 us
    all_to_all x1, waiting for transfers between devices, project_out(): lax.all_to_all(mixed.reshape(2 * tp, chips * rows, columns), ('kv', 'tp')...  3.97 us
    all_to_all x1, starting transfers between devices, project_out(): lax.all_to_all(mixed.reshape(2 * tp, chips * rows, columns), ('kv', 'tp')...  3.78 us
    ppermute x3, starting transfers between devices, passed_on(): passed.append(lax.ppermute(weight, 'tp', ring(tp, step)))  3.44 us
  transfers between devices with their start and end apart: 9, of which 3 were waited for; matrix products, arithmetic and copies ran while one was open for 0% of the time, Pallas kernels for 9%

profile of v6, /device:TPU:1, one launch (start us, length us, event | category | flops | bytes accessed | tf_op | source)
XLA Modules:
  0.0 59.6 jit_solution(753353290710628495)
XLA Ops:
  0.6 0.0 copy-start
  0.6 10.2 %shard_map.216 = (bf16[16,64,512]{2,1,0:T(8,128)(2,1)}, bf16[64,512]{1,0:T(8,128)(2,1)}, bf16[64,512]{1,0:T(8,128)(2,1)}, f32[32,64]{1,0:T(8,128)}) custom-call(s32[16]{0:T(128)} %accepted.3, bf16[16,4,4096]{2,1,0:T(4,128)(2,1)} %tokens.1, bf16[4096]{0:T(1024)(128)(2,1)} %norm_gain.1, bf16[4096,512]{1,0:T(8,128)(2,1)} %query_weight.1, ...), custom_call_target="tpu_custom_call" | custom-call | flops 1073741824 | bytes 23068672 | tf_op jit(solution)/shard_map/pallas_call | solution.py:453
  10.8 12.0 %all-to-all-start = ((bf16[64,16,512]{2,1,0:T(8,128)(2,1)}), bf16[64,16,512]{2,1,0:T(8,128)(2,1)S(1)}, u32[]{:S(2)}, u32[]{:S(2)}) async-start(bf16[64,16,512]{2,1,0:T(8,128)(2,1)} %bitcast.14), calls=%async_computation | async-start | bytes 2097152 | tf_op jit(solution)/shard_map/all_to_all | solution.py:67
  22.8 0.0 copy-done
  22.8 2.3 %collective-permute-start.2 = (bf16[512,128]{1,0:T(8,128)(2,1)S(1)}, bf16[512,128]{1,0:T(8,128)(2,1)S(1)}, u32[]{:S(2)}, u32[]{:S(2)}) collective-permute-start(bf16[512,128]{1,0:T(8,128)(2,1)S(1)} %copy-done), channel_id=1, source_target_pairs={{0,3},{1,0},{2,1},{3,2},{4,7},{5,4},{6,5},{7,6},{8,11},{9,8},{10,9... | collective-permute-start | bytes 393224 | tf_op jit(solution)/shard_map/ppermute | solution.py:25
  25.1 0.6 collective-permute-start.1
  25.7 0.6 collective-permute-start
  26.2 2.1 %collective-permute-start.3 = (bf16[512,128]{1,0:T(8,128)(2,1)S(1)}, bf16[512,128]{1,0:T(8,128)(2,1)S(1)}, u32[]{:S(2)}, u32[]{:S(2)}) collective-permute-start(bf16[512,128]{1,0:T(8,128)(2,1)S(1)} %copy-done), channel_id=1, source_target_pairs={{0,4},{4,0},{8,12},{12,8},{16,20},{20,16},{24,28},{28,24},{32,36},... | collective-permute-start | bytes 393224 | tf_op jit(solution)/shard_map/ppermute | solution.py:18
  28.3 9.2 %collective-permute-done.2.refs_3_ = bf16[512,128]{1,0:T(8,128)(2,1)S(1)} collective-permute-done((bf16[512,128]{1,0:T(8,128)(2,1)S(1)}, bf16[512,128]{1,0:T(8,128)(2,1)S(1)}, u32[]{:S(2)}, u32[]{:S(2)}) %collective-permute-start.2) | collective-permute-done | bytes 131104 | tf_op jit(solution)/shard_map/ppermute | solution.py:25
  37.5 3.2 %collective-permute-start.6 = (bf16[512,128]{1,0:T(8,128)(2,1)S(1)}, bf16[512,128]{1,0:T(8,128)(2,1)S(1)}, u32[]{:S(2)}, u32[]{:S(2)}) collective-permute-start(bf16[512,128]{1,0:T(8,128)(2,1)S(1)} %collective-permute-done.2.refs_3_), channel_id=1, source_target_pairs={{0,4},{4,0},{8,12},{12,8},{16,20},{20,16},{24,28},{28,24},{32,36},... | collective-permute-start | bytes 393224 | tf_op jit(solution)/shard_map/ppermute | solution.py:18
  40.7 0.0 collective-permute-done.1.refs_2_
  40.7 1.5 %collective-permute-start.5 = (bf16[512,128]{1,0:T(8,128)(2,1)S(1)}, bf16[512,128]{1,0:T(8,128)(2,1)S(1)}, u32[]{:S(2)}, u32[]{:S(2)}) collective-permute-start(bf16[512,128]{1,0:T(8,128)(2,1)S(1)} %collective-permute-done.1.refs_2_), channel_id=1, source_target_pairs={{0,4},{4,0},{8,12},{12,8},{16,20},{20,16},{24,28},{28,24},{32,36},... | collective-permute-start | bytes 393224 | tf_op jit(solution)/shard_map/ppermute | solution.py:18
  42.2 0.0 collective-permute-done.refs_1_
  42.2 1.1 %collective-permute-start.4 = (bf16[512,128]{1,0:T(8,128)(2,1)S(1)}, bf16[512,128]{1,0:T(8,128)(2,1)S(1)}, u32[]{:S(2)}, u32[]{:S(2)}) collective-permute-start(bf16[512,128]{1,0:T(8,128)(2,1)S(1)} %collective-permute-done.refs_1_), channel_id=1, source_target_pairs={{0,4},{4,0},{8,12},{12,8},{16,20},{20,16},{24,28},{28,24},{32,36},... | collective-permute-start | bytes 393224 | tf_op jit(solution)/shard_map/ppermute | solution.py:18
  43.3 0.0 collective-permute-done.3.refs_4_
  43.3 0.0 collective-permute-done.6.refs_7_
  43.3 0.0 collective-permute-done.5.refs_6_
  43.3 1.0 %collective-permute-done.4.refs_5_ = bf16[512,128]{1,0:T(8,128)(2,1)S(1)} collective-permute-done((bf16[512,128]{1,0:T(8,128)(2,1)S(1)}, bf16[512,128]{1,0:T(8,128)(2,1)S(1)}, u32[]{:S(2)}, u32[]{:S(2)}) %collective-permute-start.4) | collective-permute-done | bytes 131104 | tf_op jit(solution)/shard_map/ppermute | solution.py:18
  44.3 0.0 all-to-all-done
  44.3 1.2 %shard_map.217 = bf16[2,4,256,128]{3,2,1,0:T(8,128)(2,1)} custom-call(bf16[16,4,16,512]{3,2,1,0:T(8,128)(2,1)S(1)} %bitcast.12, bf16[512,128]{1,0:T(8,128)(2,1)S(1)} %copy-done, bf16[512,128]{1,0:T(8,128)(2,1)S(1)} %collective-permute-done.refs_1_, bf16[512,128]{1,0:T(8,128)(2,1)S(1)} %collective-permute-done.1.refs_2_, ...), custom_call_target="tpu_custom_call" | custom-call | flops 268435456 | bytes 3145728 | tf_op jit(solution)/shard_map/pallas_call | solution.py:72
  45.6 3.8 %all-to-all-start.1 = ((bf16[8,256,128]{2,1,0:T(8,128)(2,1)}), bf16[8,256,128]{2,1,0:T(8,128)(2,1)S(1)}, u32[]{:S(2)}, u32[]{:S(2)}) async-start(bf16[8,256,128]{2,1,0:T(8,128)(2,1)} %bitcast.5), calls=%async_computation.1 | async-start | bytes 1048576 | tf_op jit(solution)/shard_map/all_to_all | solution.py:82
  49.3 5.4 %shard_map.218 = (f32[16,4,128,128]{3,2,1,0:T(8,128)}, f32[16,4,128]{2,1,0:T(4,128)}, f32[4,16]{1,0:T(4,128)}, bf16[16,4,4,128]{3,2,1,0:T(4,128)(2,1)}, bf16[16,...) custom-call(s32[16]{0:T(128)} %accepted.3, f32[16,4,128,128]{3,2,1,0:T(8,128)} %state_c.3, f32[16,4,128]{2,1,0:T(4,128)} %state_n.3, ...), custom_call_target="tpu_custom_call" | custom-call | flops 134217728 | bytes 9437184 | tf_op jit(solution)/shard_map/pallas_call | solution.py:493
  54.7 4.0 %all-to-all-done.1 = bf16[8,256,128]{2,1,0:T(8,128)(2,1)S(1)} async-done(((bf16[8,256,128]{2,1,0:T(8,128)(2,1)}), bf16[8,256,128]{2,1,0:T(8,128)(2,1)S(1)}, u32[]{:S(2)}, u32[]{:S(2)}) %all-to-all-start.1) | async-done | bytes 524320 | tf_op jit(solution)/shard_map/all_to_all | solution.py:82
  58.7 0.9 %copy.24 = bf16[2,4,16,16,128]{4,3,1,0,2:T(8,128)(2,1)} copy(bf16[2,4,16,16,128]{4,3,2,1,0:T(8,128)(2,1)S(1)} %bitcast.13) | data formatting | bytes 1048576 | tf_op jit(solution)/shard_map/reshape | solution.py:85
Async XLA Ops:
  0.6 22.1 %copy-start = (bf16[512,128]{1,0:T(8,128)(2,1)S(1)}, bf16[512,128]{1,0:T(8,128)(2,1)}, u32[]{:S(2)}) copy-start(bf16[512,128]{1,0:T(8,128)(2,1)} %refs_0_.1) | copy-start | bytes 393220
  10.8 33.5 %all-to-all-start = ((bf16[64,16,512]{2,1,0:T(8,128)(2,1)}), bf16[64,16,512]{2,1,0:T(8,128)(2,1)S(1)}, u32[]{:S(2)}, u32[]{:S(2)}) async-start(bf16[64,16,512]{2,1,0:T(8,128)(2,1)} %bitcast.14), calls=%async_computation | async-start | bytes 2097152 | tf_op jit(solution)/shard_map/all_to_all | solution.py:67
  22.8 14.7 %collective-permute-start.2 = (bf16[512,128]{1,0:T(8,128)(2,1)S(1)}, bf16[512,128]{1,0:T(8,128)(2,1)S(1)}, u32[]{:S(2)}, u32[]{:S(2)}) collective-permute-start(bf16[512,128]{1,0:T(8,128)(2,1)S(1)} %copy-done), channel_id=1, source_target_pairs={{0,3},{1,0},{2,1},{3,2},{4,7},{5,4},{6,5},{7,6},{8,11},{9,8},{10,9... | collective-permute-start | bytes 393224 | tf_op jit(solution)/shard_map/ppermute | solution.py:25
  25.1 15.6 %collective-permute-start.1 = (bf16[512,128]{1,0:T(8,128)(2,1)S(1)}, bf16[512,128]{1,0:T(8,128)(2,1)S(1)}, u32[]{:S(2)}, u32[]{:S(2)}) collective-permute-start(bf16[512,128]{1,0:T(8,128)(2,1)S(1)} %copy-done), channel_id=1, source_target_pairs={{0,2},{1,3},{2,0},{3,1},{4,6},{5,7},{6,4},{7,5},{8,10},{9,11},{10,... | collective-permute-start | bytes 393224 | tf_op jit(solution)/shard_map/ppermute | solution.py:25
  25.7 16.6 %collective-permute-start = (bf16[512,128]{1,0:T(8,128)(2,1)S(1)}, bf16[512,128]{1,0:T(8,128)(2,1)S(1)}, u32[]{:S(2)}, u32[]{:S(2)}) collective-permute-start(bf16[512,128]{1,0:T(8,128)(2,1)S(1)} %copy-done), channel_id=1, source_target_pairs={{0,1},{1,2},{2,3},{3,0},{4,5},{5,6},{6,7},{7,4},{8,9},{9,10},{10,1... | collective-permute-start | bytes 393224 | tf_op jit(solution)/shard_map/ppermute | solution.py:25
  26.2 17.1 %collective-permute-start.3 = (bf16[512,128]{1,0:T(8,128)(2,1)S(1)}, bf16[512,128]{1,0:T(8,128)(2,1)S(1)}, u32[]{:S(2)}, u32[]{:S(2)}) collective-permute-start(bf16[512,128]{1,0:T(8,128)(2,1)S(1)} %copy-done), channel_id=1, source_target_pairs={{0,4},{4,0},{8,12},{12,8},{16,20},{20,16},{24,28},{28,24},{32,36},... | collective-permute-start | bytes 393224 | tf_op jit(solution)/shard_map/ppermute | solution.py:18
  37.5 5.8 %collective-permute-start.6 = (bf16[512,128]{1,0:T(8,128)(2,1)S(1)}, bf16[512,128]{1,0:T(8,128)(2,1)S(1)}, u32[]{:S(2)}, u32[]{:S(2)}) collective-permute-start(bf16[512,128]{1,0:T(8,128)(2,1)S(1)} %collective-permute-done.2.refs_3_), channel_id=1, source_target_pairs={{0,4},{4,0},{8,12},{12,8},{16,20},{20,16},{24,28},{28,24},{32,36},... | collective-permute-start | bytes 393224 | tf_op jit(solution)/shard_map/ppermute | solution.py:18
  40.7 2.6 %collective-permute-start.5 = (bf16[512,128]{1,0:T(8,128)(2,1)S(1)}, bf16[512,128]{1,0:T(8,128)(2,1)S(1)}, u32[]{:S(2)}, u32[]{:S(2)}) collective-permute-start(bf16[512,128]{1,0:T(8,128)(2,1)S(1)} %collective-permute-done.1.refs_2_), channel_id=1, source_target_pairs={{0,4},{4,0},{8,12},{12,8},{16,20},{20,16},{24,28},{28,24},{32,36},... | collective-permute-start | bytes 393224 | tf_op jit(solution)/shard_map/ppermute | solution.py:18
  42.2 2.1 %collective-permute-start.4 = (bf16[512,128]{1,0:T(8,128)(2,1)S(1)}, bf16[512,128]{1,0:T(8,128)(2,1)S(1)}, u32[]{:S(2)}, u32[]{:S(2)}) collective-permute-start(bf16[512,128]{1,0:T(8,128)(2,1)S(1)} %collective-permute-done.refs_1_), channel_id=1, source_target_pairs={{0,4},{4,0},{8,12},{12,8},{16,20},{20,16},{24,28},{28,24},{32,36},... | collective-permute-start | bytes 393224 | tf_op jit(solution)/shard_map/ppermute | solution.py:18
  45.6 13.1 %all-to-all-start.1 = ((bf16[8,256,128]{2,1,0:T(8,128)(2,1)}), bf16[8,256,128]{2,1,0:T(8,128)(2,1)S(1)}, u32[]{:S(2)}, u32[]{:S(2)}) async-start(bf16[8,256,128]{2,1,0:T(8,128)(2,1)} %bitcast.5), calls=%async_computation.1 | async-start | bytes 1048576 | tf_op jit(solution)/shard_map/all_to_all | solution.py:82

commit v7 on v6

--- a/solution.py
+++ b/solution.py
@@ -209,6 +209,9 @@
     keys_v,
     values_v,
     gates_v,
+    decay_v,
+    replayed_v,
+    both_v,
     sems,
     out_sems,
 ):
@@ -289,13 +292,39 @@
                 preferred_element_type=f32,
             )
             acc = part if acc is None else acc + part
-        return acc.astype(bf16)
-
-    queries = project(0)
+        return acc
+
+    queries = project(0).astype(bf16)
+
+    def before(h):
+        cols = slice(h * size, (h + 1) * size)
+        query = queries[:, cols]
+        old_key = prev_keys_v[:, h].astype(f32).reshape(rows, size).astype(bf16)
+        c_col = cumul[:, heads_total + h : heads_total + h + 1]
+        c_row = cumul_t[heads_total + h : heads_total + h + 1, :]
+        i_row = gates_t[h : h + 1, :]
+        logs_ts = jnp.where(causal, c_col - c_row + i_row, -jnp.inf)
+        carried = c_col + stable_col[:, h : h + 1]
+        steady = jnp.maximum(carried, jnp.max(logs_ts, axis=1, keepdims=True))
+        weight_state = jnp.exp(carried - steady)
+        decay_v[h] = scale * jnp.exp(logs_ts - steady)
+        replayed = jnp.where(same, dot_nt(query, old_key) * weights[h : h + 1, :], 0.0)
+        replayed = weight_state * replayed
+        replayed_v[h] = replayed
+        kept = weight_state * shrink_col[:, h : h + 1]
+        along = exact_dot(query.astype(f32), state_n_v[:, h, :], (1, 1))
+        denom = kept * jnp.sum(along * down, axis=1, keepdims=True)
+        denom = denom + jnp.sum(replayed, axis=1, keepdims=True)
+        return kept, denom, jnp.exp(-steady)
+
     upper = iota((2 * props, size), 0) < props
+    starts = []
+    firsts = [before(h) for h in range(heads)]
     for h in range(heads):
         cols = slice(h * size, (h + 1) * size)
         query_f = queries[:, cols].astype(f32)
+        kept, denom, least = firsts[h]
+        starts.append((denom, least))
         states_in[h].wait()
         for p in range(seqs // 2):
             stacked = [
@@ -305,45 +334,40 @@
             asked = query_f[pair].astype(bf16)
             found = dot_nt(asked, jnp.concatenate(stacked, axis=0))
             recall_v[pair, cols] = jnp.where(upper, found[:, :size], found[:, size:])
-
-    new_keys = project(1)
+        recall_v[:, cols] = kept * recall_v[:, cols]
+
+    new_keys = project(1).astype(bf16)
     keys_v[...] = new_keys
     sends.append(pltpu.make_async_copy(keys_v, keys_out, out_sems.at[1]))
     sends[1].start()
-    new_values = project(2)
+    ready = []
+    for h in range(heads):
+        cols = slice(h * size, (h + 1) * size)
+        scores = dot_nt(queries[:, cols], new_keys[:, cols]) * decay_v[h]
+        denom, least = starts[h]
+        denom = denom + jnp.sum(scores, axis=1, keepdims=True)
+        ready.append(1.0 / jnp.maximum(jnp.abs(denom), least))
+        both_v[h] = jnp.concatenate(
+            split(jnp.concatenate([replayed_v[h], scores], axis=1)), axis=1
+        )
+    new_values = project(2).astype(bf16)
     values_v[...] = new_values
     sends.append(pltpu.make_async_copy(values_v, values_out, out_sems.at[2]))
     sends[2].start()
     for h in range(heads):
         cols = slice(h * size, (h + 1) * size)
-        query, key, value = queries[:, cols], new_keys[:, cols], new_values[:, cols]
-        old_key = prev_keys_v[:, h].astype(f32).reshape(rows, size).astype(bf16)
         old_value = prev_values_v[:, h].astype(f32).reshape(rows, size).astype(bf16)
-        c_col = cumul[:, heads_total + h : heads_total + h + 1]
-        c_row = cumul_t[heads_total + h : heads_total + h + 1, :]
-        i_row = gates_t[h : h + 1, :]
-        logs_ts = jnp.where(causal, c_col - c_row + i_row, -jnp.inf)
-        carried = c_col + stable_col[:, h : h + 1]
-        steady = jnp.maximum(carried, jnp.max(logs_ts, axis=1, keepdims=True))
-        weight_state = jnp.exp(carried - steady)
-        scores = dot_nt(query, key) * scale * jnp.exp(logs_ts - steady)
-        replayed = jnp.where(same, dot_nt(query, old_key) * weights[h : h + 1, :], 0.0)
-        both = jnp.concatenate([weight_state * replayed, scores], axis=1)
-        kept = weight_state * shrink_col[:, h : h + 1]
-        numer = kept * recall_v[:, cols] + jnp.dot(
-            jnp.concatenate(split(both), axis=1),
-            jnp.concatenate([old_value, value] * 2, axis=0),
+        numer = recall_v[:, cols] + jnp.dot(
+            both_v[h],
+            jnp.concatenate([old_value, new_values[:, cols]] * 2, axis=0),
             preferred_element_type=f32,
         )
-        along = exact_dot(query.astype(f32), state_n_v[:, h, :], (1, 1))
-        recall_norm = jnp.sum(along * down, axis=1, keepdims=True)
-        denom = kept * recall_norm + jnp.sum(both, axis=1, keepdims=True)
-        hidden = numer / jnp.maximum(jnp.abs(denom), jnp.exp(-steady))
+        hidden = numer * ready[h]
         hidden_v[:, cols] = hidden * lax.rsqrt(
             jnp.mean(hidden * hidden, axis=1, keepdims=True) + EPSILON
         )
 
-    outgate = project(3)
+    outgate = project(3).astype(bf16)
     head_scale = head_gain_v[...].astype(f32).reshape(1, heads * size)
     gated_v[...] = (
         hidden_v[...] * head_scale * jax.nn.sigmoid(outgate.astype(f32))
@@ -482,6 +506,9 @@
             pltpu.VMEM((rows, columns), bf16),
             pltpu.VMEM((rows, columns), bf16),
             pltpu.VMEM((gate_weight.shape[1], rows), f32),
+            pltpu.VMEM((heads, rows, rows), f32),
+            pltpu.VMEM((heads, rows, rows), f32),
+            pltpu.VMEM((heads, rows, 4 * rows), bf16),
             pltpu.SemaphoreType.DMA((11 + 16 + heads,)),
             pltpu.SemaphoreType.DMA((3 + chips,)),
         ],

time: 59.9 us -> 59.9 us (level)
  no operation moved by 1% of the time
where the time goes in v7:
time: 59.9 us; the launch traced here: 59.6 us
  starting transfers between devices  27.1 us (45%)
  Pallas kernels  16.8 us (28%)
  waiting for transfers between devices  14.2 us (24%)
  local copies, waits for them, and re-layouts  0.86 us (1%)
  between operations  0.69 us (1%)
    all_to_all x1, starting transfers between devices, project_out(): lax.all_to_all(sent.reshape(chips * tp, rows, depth), ('kv', 'tp'), 0, 0,...  12 us
    pallas_call x1, Pallas kernels, cell(): pl.pallas_call(cell_kernel, out_shape=(jax.ShapeDtypeStruct((chips, rows,...  10.2 us
    ppermute x3, waiting for transfers between devices, passed_on(): passed.append(lax.ppermute(weight, 'tp', ring(tp, step)))  9.2 us
    ppermute x4, starting transfers between devices, swap_cores(): lax.ppermute(x, 'kv', [(i, i ^ 1) for i in range(lax.axis_size('kv'))])  7.9 us
    pallas_call x1, Pallas kernels, cell(): pl.pallas_call(keep_kernel, out_shape=(jax.ShapeDtypeStruct(state_c.shape...  5.38 us
    all_to_all x1, waiting for transfers between devices, project_out(): lax.all_to_all(mixed.reshape(2 * tp, chips * rows, columns), ('kv', 'tp')...  3.97 us
    all_to_all x1, starting transfers between devices, project_out(): lax.all_to_all(mixed.reshape(2 * tp, chips * rows, columns), ('kv', 'tp')...  3.78 us
    ppermute x3, starting transfers between devices, passed_on(): passed.append(lax.ppermute(weight, 'tp', ring(tp, step)))  3.44 us
  transfers between devices with their start and end apart: 9, of which 3 were waited for; matrix products, arithmetic and copies ran while one was open for 0% of the time, Pallas kernels for 9%

profile of v7, /device:TPU:1, one launch (start us, length us, event | category | flops | bytes accessed | tf_op | source)
XLA Modules:
  0.0 59.6 jit_solution(14515685891400123917)
XLA Ops:
  0.6 0.0 copy-start
  0.6 10.2 %shard_map.216 = (bf16[16,64,512]{2,1,0:T(8,128)(2,1)}, bf16[64,512]{1,0:T(8,128)(2,1)}, bf16[64,512]{1,0:T(8,128)(2,1)}, f32[32,64]{1,0:T(8,128)}) custom-call(s32[16]{0:T(128)} %accepted.3, bf16[16,4,4096]{2,1,0:T(4,128)(2,1)} %tokens.1, bf16[4096]{0:T(1024)(128)(2,1)} %norm_gain.1, bf16[4096,512]{1,0:T(8,128)(2,1)} %query_weight.1, ...), custom_call_target="tpu_custom_call" | custom-call | flops 1073741824 | bytes 23068672 | tf_op jit(solution)/shard_map/pallas_call | solution.py:477
  10.8 12.0 %all-to-all-start = ((bf16[64,16,512]{2,1,0:T(8,128)(2,1)}), bf16[64,16,512]{2,1,0:T(8,128)(2,1)S(1)}, u32[]{:S(2)}, u32[]{:S(2)}) async-start(bf16[64,16,512]{2,1,0:T(8,128)(2,1)} %bitcast.14), calls=%async_computation | async-start | bytes 2097152 | tf_op jit(solution)/shard_map/all_to_all | solution.py:67
  22.8 0.0 copy-done
  22.8 2.3 %collective-permute-start.2 = (bf16[512,128]{1,0:T(8,128)(2,1)S(1)}, bf16[512,128]{1,0:T(8,128)(2,1)S(1)}, u32[]{:S(2)}, u32[]{:S(2)}) collective-permute-start(bf16[512,128]{1,0:T(8,128)(2,1)S(1)} %copy-done), channel_id=1, source_target_pairs={{0,3},{1,0},{2,1},{3,2},{4,7},{5,4},{6,5},{7,6},{8,11},{9,8},{10,9... | collective-permute-start | bytes 393224 | tf_op jit(solution)/shard_map/ppermute | solution.py:25
  25.1 0.6 collective-permute-start.1
  25.7 0.6 collective-permute-start
  26.3 2.1 %collective-permute-start.3 = (bf16[512,128]{1,0:T(8,128)(2,1)S(1)}, bf16[512,128]{1,0:T(8,128)(2,1)S(1)}, u32[]{:S(2)}, u32[]{:S(2)}) collective-permute-start(bf16[512,128]{1,0:T(8,128)(2,1)S(1)} %copy-done), channel_id=1, source_target_pairs={{0,4},{4,0},{8,12},{12,8},{16,20},{20,16},{24,28},{28,24},{32,36},... | collective-permute-start | bytes 393224 | tf_op jit(solution)/shard_map/ppermute | solution.py:18
  28.3 9.2 %collective-permute-done.2.refs_3_ = bf16[512,128]{1,0:T(8,128)(2,1)S(1)} collective-permute-done((bf16[512,128]{1,0:T(8,128)(2,1)S(1)}, bf16[512,128]{1,0:T(8,128)(2,1)S(1)}, u32[]{:S(2)}, u32[]{:S(2)}) %collective-permute-start.2) | collective-permute-done | bytes 131104 | tf_op jit(solution)/shard_map/ppermute | solution.py:25
  37.5 3.2 %collective-permute-start.6 = (bf16[512,128]{1,0:T(8,128)(2,1)S(1)}, bf16[512,128]{1,0:T(8,128)(2,1)S(1)}, u32[]{:S(2)}, u32[]{:S(2)}) collective-permute-start(bf16[512,128]{1,0:T(8,128)(2,1)S(1)} %collective-permute-done.2.refs_3_), channel_id=1, source_target_pairs={{0,4},{4,0},{8,12},{12,8},{16,20},{20,16},{24,28},{28,24},{32,36},... | collective-permute-start | bytes 393224 | tf_op jit(solution)/shard_map/ppermute | solution.py:18
  40.7 0.0 collective-permute-done.1.refs_2_
  40.7 1.5 %collective-permute-start.5 = (bf16[512,128]{1,0:T(8,128)(2,1)S(1)}, bf16[512,128]{1,0:T(8,128)(2,1)S(1)}, u32[]{:S(2)}, u32[]{:S(2)}) collective-permute-start(bf16[512,128]{1,0:T(8,128)(2,1)S(1)} %collective-permute-done.1.refs_2_), channel_id=1, source_target_pairs={{0,4},{4,0},{8,12},{12,8},{16,20},{20,16},{24,28},{28,24},{32,36},... | collective-permute-start | bytes 393224 | tf_op jit(solution)/shard_map/ppermute | solution.py:18
  42.2 0.0 collective-permute-done.refs_1_
  42.3 1.1 %collective-permute-start.4 = (bf16[512,128]{1,0:T(8,128)(2,1)S(1)}, bf16[512,128]{1,0:T(8,128)(2,1)S(1)}, u32[]{:S(2)}, u32[]{:S(2)}) collective-permute-start(bf16[512,128]{1,0:T(8,128)(2,1)S(1)} %collective-permute-done.refs_1_), channel_id=1, source_target_pairs={{0,4},{4,0},{8,12},{12,8},{16,20},{20,16},{24,28},{28,24},{32,36},... | collective-permute-start | bytes 393224 | tf_op jit(solution)/shard_map/ppermute | solution.py:18
  43.4 0.0 collective-permute-done.3.refs_4_
  43.4 0.0 collective-permute-done.6.refs_7_
  43.4 0.0 collective-permute-done.5.refs_6_
  43.4 1.0 %collective-permute-done.4.refs_5_ = bf16[512,128]{1,0:T(8,128)(2,1)S(1)} collective-permute-done((bf16[512,128]{1,0:T(8,128)(2,1)S(1)}, bf16[512,128]{1,0:T(8,128)(2,1)S(1)}, u32[]{:S(2)}, u32[]{:S(2)}) %collective-permute-start.4) | collective-permute-done | bytes 131104 | tf_op jit(solution)/shard_map/ppermute | solution.py:18
  44.3 0.0 all-to-all-done
  44.3 1.2 %shard_map.217 = bf16[2,4,256,128]{3,2,1,0:T(8,128)(2,1)} custom-call(bf16[16,4,16,512]{3,2,1,0:T(8,128)(2,1)S(1)} %bitcast.12, bf16[512,128]{1,0:T(8,128)(2,1)S(1)} %copy-done, bf16[512,128]{1,0:T(8,128)(2,1)S(1)} %collective-permute-done.refs_1_, bf16[512,128]{1,0:T(8,128)(2,1)S(1)} %collective-permute-done.1.refs_2_, ...), custom_call_target="tpu_custom_call" | custom-call | flops 268435456 | bytes 3145728 | tf_op jit(solution)/shard_map/pallas_call | solution.py:72
  45.6 3.8 %all-to-all-start.1 = ((bf16[8,256,128]{2,1,0:T(8,128)(2,1)}), bf16[8,256,128]{2,1,0:T(8,128)(2,1)S(1)}, u32[]{:S(2)}, u32[]{:S(2)}) async-start(bf16[8,256,128]{2,1,0:T(8,128)(2,1)} %bitcast.5), calls=%async_computation.1 | async-start | bytes 1048576 | tf_op jit(solution)/shard_map/all_to_all | solution.py:82
  49.4 5.4 %shard_map.218 = (f32[16,4,128,128]{3,2,1,0:T(8,128)}, f32[16,4,128]{2,1,0:T(4,128)}, f32[4,16]{1,0:T(4,128)}, bf16[16,4,4,128]{3,2,1,0:T(4,128)(2,1)}, bf16[16,...) custom-call(s32[16]{0:T(128)} %accepted.3, f32[16,4,128,128]{3,2,1,0:T(8,128)} %state_c.3, f32[16,4,128]{2,1,0:T(4,128)} %state_n.3, ...), custom_call_target="tpu_custom_call" | custom-call | flops 134217728 | bytes 9437184 | tf_op jit(solution)/shard_map/pallas_call | solution.py:520
  54.8 4.0 %all-to-all-done.1 = bf16[8,256,128]{2,1,0:T(8,128)(2,1)S(1)} async-done(((bf16[8,256,128]{2,1,0:T(8,128)(2,1)}), bf16[8,256,128]{2,1,0:T(8,128)(2,1)S(1)}, u32[]{:S(2)}, u32[]{:S(2)}) %all-to-all-start.1) | async-done | bytes 524320 | tf_op jit(solution)/shard_map/all_to_all | solution.py:82
  58.7 0.9 %copy.24 = bf16[2,4,16,16,128]{4,3,1,0,2:T(8,128)(2,1)} copy(bf16[2,4,16,16,128]{4,3,2,1,0:T(8,128)(2,1)S(1)} %bitcast.13) | data formatting | bytes 1048576 | tf_op jit(solution)/shard_map/reshape | solution.py:85
Async XLA Ops:
  0.6 22.2 %copy-start = (bf16[512,128]{1,0:T(8,128)(2,1)S(1)}, bf16[512,128]{1,0:T(8,128)(2,1)}, u32[]{:S(2)}) copy-start(bf16[512,128]{1,0:T(8,128)(2,1)} %refs_0_.1) | copy-start | bytes 393220
  10.8 33.5 %all-to-all-start = ((bf16[64,16,512]{2,1,0:T(8,128)(2,1)}), bf16[64,16,512]{2,1,0:T(8,128)(2,1)S(1)}, u32[]{:S(2)}, u32[]{:S(2)}) async-start(bf16[64,16,512]{2,1,0:T(8,128)(2,1)} %bitcast.14), calls=%async_computation | async-start | bytes 2097152 | tf_op jit(solution)/shard_map/all_to_all | solution.py:67
  22.8 14.7 %collective-permute-start.2 = (bf16[512,128]{1,0:T(8,128)(2,1)S(1)}, bf16[512,128]{1,0:T(8,128)(2,1)S(1)}, u32[]{:S(2)}, u32[]{:S(2)}) collective-permute-start(bf16[512,128]{1,0:T(8,128)(2,1)S(1)} %copy-done), channel_id=1, source_target_pairs={{0,3},{1,0},{2,1},{3,2},{4,7},{5,4},{6,5},{7,6},{8,11},{9,8},{10,9... | collective-permute-start | bytes 393224 | tf_op jit(solution)/shard_map/ppermute | solution.py:25
  25.1 15.6 %collective-permute-start.1 = (bf16[512,128]{1,0:T(8,128)(2,1)S(1)}, bf16[512,128]{1,0:T(8,128)(2,1)S(1)}, u32[]{:S(2)}, u32[]{:S(2)}) collective-permute-start(bf16[512,128]{1,0:T(8,128)(2,1)S(1)} %copy-done), channel_id=1, source_target_pairs={{0,2},{1,3},{2,0},{3,1},{4,6},{5,7},{6,4},{7,5},{8,10},{9,11},{10,... | collective-permute-start | bytes 393224 | tf_op jit(solution)/shard_map/ppermute | solution.py:25
  25.7 16.6 %collective-permute-start = (bf16[512,128]{1,0:T(8,128)(2,1)S(1)}, bf16[512,128]{1,0:T(8,128)(2,1)S(1)}, u32[]{:S(2)}, u32[]{:S(2)}) collective-permute-start(bf16[512,128]{1,0:T(8,128)(2,1)S(1)} %copy-done), channel_id=1, source_target_pairs={{0,1},{1,2},{2,3},{3,0},{4,5},{5,6},{6,7},{7,4},{8,9},{9,10},{10,1... | collective-permute-start | bytes 393224 | tf_op jit(solution)/shard_map/ppermute | solution.py:25
  26.3 17.1 %collective-permute-start.3 = (bf16[512,128]{1,0:T(8,128)(2,1)S(1)}, bf16[512,128]{1,0:T(8,128)(2,1)S(1)}, u32[]{:S(2)}, u32[]{:S(2)}) collective-permute-start(bf16[512,128]{1,0:T(8,128)(2,1)S(1)} %copy-done), channel_id=1, source_target_pairs={{0,4},{4,0},{8,12},{12,8},{16,20},{20,16},{24,28},{28,24},{32,36},... | collective-permute-start | bytes 393224 | tf_op jit(solution)/shard_map/ppermute | solution.py:18
  37.5 5.8 %collective-permute-start.6 = (bf16[512,128]{1,0:T(8,128)(2,1)S(1)}, bf16[512,128]{1,0:T(8,128)(2,1)S(1)}, u32[]{:S(2)}, u32[]{:S(2)}) collective-permute-start(bf16[512,128]{1,0:T(8,128)(2,1)S(1)} %collective-permute-done.2.refs_3_), channel_id=1, source_target_pairs={{0,4},{4,0},{8,12},{12,8},{16,20},{20,16},{24,28},{28,24},{32,36},... | collective-permute-start | bytes 393224 | tf_op jit(solution)/shard_map/ppermute | solution.py:18
  40.7 2.6 %collective-permute-start.5 = (bf16[512,128]{1,0:T(8,128)(2,1)S(1)}, bf16[512,128]{1,0:T(8,128)(2,1)S(1)}, u32[]{:S(2)}, u32[]{:S(2)}) collective-permute-start(bf16[512,128]{1,0:T(8,128)(2,1)S(1)} %collective-permute-done.1.refs_2_), channel_id=1, source_target_pairs={{0,4},{4,0},{8,12},{12,8},{16,20},{20,16},{24,28},{28,24},{32,36},... | collective-permute-start | bytes 393224 | tf_op jit(solution)/shard_map/ppermute | solution.py:18
  42.3 2.1 %collective-permute-start.4 = (bf16[512,128]{1,0:T(8,128)(2,1)S(1)}, bf16[512,128]{1,0:T(8,128)(2,1)S(1)}, u32[]{:S(2)}, u32[]{:S(2)}) collective-permute-start(bf16[512,128]{1,0:T(8,128)(2,1)S(1)} %collective-permute-done.refs_1_), channel_id=1, source_target_pairs={{0,4},{4,0},{8,12},{12,8},{16,20},{20,16},{24,28},{28,24},{32,36},... | collective-permute-start | bytes 393224 | tf_op jit(solution)/shard_map/ppermute | solution.py:18
  45.6 13.1 %all-to-all-start.1 = ((bf16[8,256,128]{2,1,0:T(8,128)(2,1)}), bf16[8,256,128]{2,1,0:T(8,128)(2,1)S(1)}, u32[]{:S(2)}, u32[]{:S(2)}) async-start(bf16[8,256,128]{2,1,0:T(8,128)(2,1)} %bitcast.5), calls=%async_computation.1 | async-start | bytes 1048576 | tf_op jit(solution)/shard_map/all_to_all | solution.py:82
